TPU v7x, 32 devices: a whole 2x2x4 slice. The times are simulated.
32 devices in a mesh: ep: 8 (over z, y), tp: 4 (over x, core).
Axes of the slice: x: 2, y: 2, z: 4, core: 2. Of those that a mesh axis runs over, the one named last changes fastest.
Arguments:
- resid: bfloat16 [256, 2048], P('ep'), may hold values from -6 to 6
- mix_gain: bfloat16 [2048], replicated, may hold values from 0.099609375 to 1.8984375
- proj_x: bfloat16 [2048, 512], P(None, 'tp'), may hold values from -0.125 to 0.125
- proj_z: bfloat16 [2048, 512], P(None, 'tp'), may hold values from -0.125 to 0.125
- proj_b: bfloat16 [2048, 512], P(None, 'tp'), may hold values from -0.125 to 0.125
- proj_c: bfloat16 [2048, 512], P(None, 'tp'), may hold values from -0.125 to 0.125
- proj_step: bfloat16 [2048, 8], replicated, may hold values from -0.125 to 0.125
- step_bias: float32 [8], P('tp'), may hold values from -5 to -1
- decay_rate: float32 [8], P('tp'), may hold values from 1 to 16
- conv_taps: bfloat16 [3, 4, 512], P(None, None, 'tp'), may hold values from -3 to 3
- conv_state: bfloat16 [256, 3, 3, 512], P('ep', None, None, 'tp'), may hold values from -6 to 6
- scan_state: float32 [256, 8, 64, 128], P('ep', 'tp'), may hold values from -2.5 to 2.5
- inner_gain: bfloat16 [512], P('tp'), may hold values from 0.099609375 to 1.8984375
- proj_out: bfloat16 [512, 2048], P('tp'), may hold values from -0.25 to 0.25
- post_gain: bfloat16 [2048], replicated, may hold values from 0.099609375 to 1.8984375
- ffn_gain: bfloat16 [2048], replicated, may hold values from 0.099609375 to 1.8984375
- group_router: bfloat16 [2048, 2], replicated, may hold values from -0.125 to 0.125
- expert_router: bfloat16 [2048, 8], replicated, may hold values from -0.125 to 0.125
- route_experts: int32 [256, 4], P('ep'), may hold values from 0 to 7, as said below
- expert_gate: bfloat16 [8, 2048, 1024], P('ep', None, 'tp'), may hold values from -0.125 to 0.125
- expert_up: bfloat16 [8, 2048, 1024], P('ep', None, 'tp'), may hold values from -0.125 to 0.125
- expert_down: bfloat16 [8, 1024, 2048], P('ep', 'tp')
- dense_switch: bfloat16 [2048], replicated, may hold values from -0.125 to 0.125
- dense_gate: bfloat16 [2048, 2048], P('ep', 'tp'), may hold values from -0.125 to 0.125
- dense_up: bfloat16 [2048, 2048], P('ep', 'tp'), may hold values from -0.125 to 0.125
- dense_down: bfloat16 [2048, 2048], P('ep', 'tp')
- out_gain: bfloat16 [2048], P('tp'), may hold values from 0.099609375 to 1.8984375
Outputs:
- layer_out: bfloat16 [256, 2048], P('ep', 'tp')
- new_state: float32 [256, 8, 64, 128], P('ep', 'tp')
- new_conv: bfloat16 [256, 3, 3, 512], P('ep', None, None, 'tp')
Inputs may be any that keep to these rules, and one draw needn't show every extreme that they name: `route_experts`: each row names 4 different experts, all from one group of 4 consecutive expert numbers. Within each aligned block of 32 rows (the rows of one index of ep) no expert is named more than 32 times, and one expert, the same in every block, is named exactly 32 times in every block.
All inputs are finite; a program needn't handle non-finite values.
Results may differ from a plain program's by a relative error of at most 0.019.
Values may be sent and summed in bfloat16 or wider, within the bound.
A program may use at most 64 MiB of HBM per device.

v0:
```python
import functools

import jax
import jax.numpy as jnp
from jax import lax
from jax.experimental import pallas as pl
from jax.experimental.pallas import tpu as pltpu
from jax.sharding import PartitionSpec as P

norm_eps = 1e-06


def scaled_rows(values, gain):
    values = values.astype(jnp.float32)
    mean_square = jnp.mean(values * values, axis=-1, keepdims=True)
    return values * lax.rsqrt(mean_square + norm_eps) * gain.astype(jnp.float32)


def softmax_plain(logits):
    weights = jnp.exp(logits)
    return weights / jnp.sum(weights, axis=-1, keepdims=True)


def fused_kernel(
    ep,
    group_size,
    group_count,
    expert_count,
    proj_out_ref,
    resid_ref,
    mix_ref,
    post_ref,
    ffn_ref,
    expert_router_ref,
    group_router_ref,
    switch_ref,
    route_ref,
    out_gain_ref,
    inner_ref,
    proj_step_ref,
    taps_ref,
    conv_ref,
    bias_ref,
    decay_ref,
    proj_x_hbm,
    proj_z_hbm,
    proj_b_hbm,
    proj_c_hbm,
    state_hbm,
    gate_hbm,
    up_hbm,
    down_hbm,
    dense_gate_hbm,
    dense_up_hbm,
    dense_down_hbm,
    out_ref,
    new_state_hbm,
    new_conv_ref,
    proj_w,
    state_buf,
    new_state_buf,
    router_buf,
    gate_w,
    up_w,
    down_w,
    dgate,
    dup,
    ddown,
    stream_buf,
    mix_own,
    mix_peer,
    half_own,
    half_far,
    rows_buf,
    aux_buf,
    part_buf,
    part_peer,
    send_x,
    recv_x,
    send_ep,
    recv_ep,
    square_own,
    square_peer,
    local_sem,
    state_sem,
    dense_send,
    dense_recv,
    mix_send,
    mix_recv,
    rows_send,
    rows_recv,
    aux_send,
    aux_recv,
    forward_send,
    forward_recv,
    part_send,
    part_recv,
    x_send,
    x_recv,
    ep_send,
    ep_recv,
    square_send,
    square_recv,
):
    f32, bf16 = jnp.float32, jnp.bfloat16
    me = lax.axis_index("ep")
    tp = lax.axis_index("tp")
    far = tp // 2
    core = tp % 2
    beside = far * 2 + (1 - core)
    across = (1 - far) * 2 + core
    diagonal = (1 - far) * 2 + (1 - core)
    near = (beside, across, diagonal)
    seqs, width = resid_ref.shape
    quarter = width // 4
    share = dgate.shape[1]

    def remote(src, dst, send, recv, ep_to, tp_to):
        return pltpu.make_async_remote_copy(
            src_ref=src,
            dst_ref=dst,
            send_sem=send,
            recv_sem=recv,
            device_id=(ep_to, tp_to),
            device_id_type=pl.DeviceIdType.MESH,
        )

    def ep_at(step):
        return lax.rem(me + step + ep, ep)

    local = []

    def load(src, dst):
        copy = pltpu.make_async_copy(src, dst, local_sem.at[len(local)])
        copy.start()
        local.append(copy)

    for k, src in enumerate((proj_x_hbm, proj_b_hbm, proj_c_hbm, proj_z_hbm)):
        load(src, proj_w.at[k])
    load(state_hbm, state_buf)
    load(gate_hbm.at[0], gate_w)
    load(up_hbm.at[0], up_w)
    for q in range(4):
        load(down_hbm.at[0, :, pl.ds(q * quarter, quarter)], down_w.at[q])
    dense_pairs = ((dense_gate_hbm, dgate), (dense_up_hbm, dup), (dense_down_hbm, ddown))
    for src, dst in dense_pairs:
        load(src.at[pl.ds(tp * share, share), :], dst.at[tp])

    barrier = pltpu.get_barrier_semaphore()
    for step in range(1, ep):
        pl.semaphore_signal(
            barrier, inc=1, device_id=(ep_at(step), tp), device_id_type=pl.DeviceIdType.MESH
        )
    for peer in near:
        pl.semaphore_signal(
            barrier, inc=1, device_id=(me, peer), device_id_type=pl.DeviceIdType.MESH
        )

    def row(ref):
        return ref[...].astype(f32).reshape(1, ref.shape[0])

    resid_f = resid_ref[...].astype(f32)
    resid_scale = lax.rsqrt(jnp.mean(resid_f * resid_f, axis=1, keepdims=True) + norm_eps)
    normed = (resid_f * resid_scale * row(mix_ref)).astype(bf16)
    group_base = -(-expert_count // 8) * 8
    switch_lane = group_base + -(-group_count // 8) * 8
    router_buf[...] = jnp.zeros_like(router_buf)
    router_buf[0:expert_count, :] = expert_router_ref[...].astype(f32)
    router_buf[group_base : group_base + group_count, :] = group_router_ref[...].astype(f32)
    router_buf[switch_lane : switch_lane + 1, :] = row(switch_ref)
    nt = (((1,), (1,)), ((), ()))
    step_all = lax.dot_general(normed, proj_step_ref[...], nt, preferred_element_type=f32)
    pl.semaphore_wait(barrier, ep - 1 + 3)

    sends = []
    dense_copies = []
    for t, (src, dst) in enumerate(dense_pairs):
        for k, peer in enumerate(near):
            copy = remote(
                src.at[pl.ds(peer * share, share), :],
                dst.at[tp],
                dense_send.at[3 * t + k],
                dense_recv.at[3 * t + k],
                me,
                peer,
            )
            copy.start()
            dense_copies.append(copy)
    sends += dense_copies

    channels = conv_ref.shape[3]
    heads = bias_ref.shape[0]
    head_dim = channels // heads
    taps = taps_ref[...].astype(f32)
    old = conv_ref.shape[1]
    active = []
    for k in range(3):
        local[k].wait()
        fresh = jnp.dot(normed, proj_w[k], preferred_element_type=f32).astype(bf16)
        summed = conv_ref[k, 0].astype(f32) * taps[k, 0:1]
        for tap in range(1, old):
            earlier = conv_ref[k, tap]
            new_conv_ref[k, tap - 1] = earlier
            summed = summed + earlier.astype(f32) * taps[k, tap : tap + 1]
        new_conv_ref[k, old - 1] = fresh
        summed = summed + fresh.astype(f32) * taps[k, old : old + 1]
        active.append(summed * jax.nn.sigmoid(summed))
    inputs, vec_in, vec_read = active
    local[3].wait()
    gate_z = jnp.dot(normed, proj_w[3], preferred_element_type=f32)
    step_lane = lax.broadcasted_iota(jnp.int32, step_all.shape, 1)
    lane_in = lax.broadcasted_iota(jnp.int32, (seqs, channels), 1)
    keep = jnp.zeros((seqs, channels), f32)
    stepped = jnp.zeros((seqs, channels), f32)
    for h in range(heads):
        raw = jnp.sum(
            jnp.where(step_lane == tp * heads + h, step_all, 0.0), axis=1, keepdims=True
        )
        raw = raw + bias_ref[h]
        step = jnp.maximum(raw, 0.0) + jnp.log1p(jnp.exp(-jnp.abs(raw)))
        mine = (lane_in >= h * head_dim) & (lane_in < (h + 1) * head_dim)
        keep = jnp.where(mine, jnp.exp(-decay_ref[h] * step), keep)
        stepped = jnp.where(mine, step, stepped)
    columns = jnp.concatenate(
        [keep, stepped * inputs, jnp.zeros((channels - 2 * seqs, channels), f32)], axis=0
    ).T
    local[4].wait()
    read_lane = lax.broadcasted_iota(jnp.int32, (channels, channels), 1)
    read = jnp.zeros((channels, channels), f32)
    for t in range(seqs):
        fresh_state = (
            columns[:, t : t + 1] * state_buf[t]
            + columns[:, seqs + t : seqs + t + 1] * vec_in[t : t + 1]
        )
        new_state_buf[t] = fresh_state
        value = jnp.sum(fresh_state * vec_read[t : t + 1], axis=1, keepdims=True)
        read = jnp.where(read_lane == t, value, read)
    read = read.T[0:seqs]
    gated = (read * (gate_z * jax.nn.sigmoid(gate_z)) * row(inner_ref)).astype(bf16)
    mix_own[...] = jnp.dot(gated, proj_out_ref[...], preferred_element_type=f32).astype(bf16)

    first = remote(mix_own, mix_peer, mix_send.at[0], mix_recv.at[0], me, beside)
    first.start()
    sends.append(first)
    first.wait_recv()
    half = width // 2
    chip_sum = (mix_own[...].astype(f32) + mix_peer[...].astype(f32)).astype(bf16)
    half_own[0] = chip_sum[:, :half]
    half_own[1] = chip_sum[:, half:]
    halves = []
    for k, peer in enumerate((across, diagonal)):
        copy = remote(
            half_own.at[core],
            half_far.at[core],
            mix_send.at[1 + k],
            mix_recv.at[1 + k],
            me,
            peer,
        )
        copy.start()
        halves.append(copy)
    sends += halves

    state_out = pltpu.make_async_copy(new_state_buf, new_state_hbm, state_sem)
    state_out.start()
    for copy in halves:
        copy.wait_recv()

    far_sum = jnp.concatenate([half_far[0], half_far[1]], axis=1)
    mixed = chip_sum.astype(f32) + far_sum.astype(f32)
    mixed_scale = lax.rsqrt(jnp.mean(mixed * mixed, axis=1, keepdims=True) + norm_eps)
    stream = (
        resid_f + mixed * mixed_scale * row(post_ref)
    ).astype(bf16)
    stream_f = stream.astype(f32)
    feed_scale = lax.rsqrt(jnp.mean(stream_f * stream_f, axis=1, keepdims=True) + norm_eps)
    feed = (stream_f * feed_scale * row(ffn_ref)).astype(bf16)
    for q in range(4):
        rows_buf[q, 0] = feed[:, q * quarter : (q + 1) * quarter]
        stream_buf[q] = stream[:, q * quarter : (q + 1) * quarter]

    rows_copies = []
    for step in range(1, ep):
        copy = remote(
            rows_buf.at[tp, 0],
            rows_buf.at[tp, step],
            rows_send.at[step],
            rows_recv.at[step],
            ep_at(step),
            tp,
        )
        copy.start()
        rows_copies.append(copy)
    sends += rows_copies

    logits = lax.dot_general(
        feed, router_buf[...].astype(bf16), nt, preferred_element_type=f32
    )
    lane = lax.broadcasted_iota(jnp.int32, logits.shape, 1)
    same = lax.broadcasted_iota(jnp.int32, (seqs, seqs), 0) == lax.broadcasted_iota(
        jnp.int32, (seqs, seqs), 1
    )
    route = lax.dot_general(
        jnp.where(same, 1.0, 0.0).astype(bf16),
        route_ref[...].astype(f32).astype(bf16),
        nt,
        preferred_element_type=f32,
    ).astype(jnp.int32)
    picked = lane == route[:, 0:1]
    for k in range(1, route.shape[1]):
        picked = picked | (lane == route[:, k : k + 1])
    weights = jnp.exp(logits)
    pick = jnp.where(picked, weights, 0.0)
    group_lane = (lane - group_base) * group_size
    in_groups = (lane >= group_base) & (lane < group_base + group_count)
    group = jnp.where(in_groups, weights, 0.0)
    lead = route[:, 0:1]
    chosen = in_groups & (lead >= group_lane) & (lead < group_lane + group_size)
    group_weight = jnp.sum(jnp.where(chosen, weights, 0.0), axis=1, keepdims=True) / jnp.sum(
        group, axis=1, keepdims=True
    )
    pick = pick / jnp.sum(pick, axis=1, keepdims=True) * group_weight
    aux_buf[0] = jnp.where(lane == switch_lane, jax.nn.sigmoid(logits), pick).astype(bf16)
    aux_copies = []
    for step in range(1, ep):
        copy = remote(
            aux_buf.at[0],
            aux_buf.at[step],
            aux_send.at[step],
            aux_recv.at[step],
            ep_at(step),
            tp,
        )
        copy.start()
        aux_copies.append(copy)
    sends += aux_copies

    to_beside, to_across, to_last = [], [], []
    for step in range(1, ep):
        rows_copies[step - 1].wait_recv()
        for k, (peer, kept) in enumerate(((across, to_across), (beside, to_beside))):
            copy = remote(
                rows_buf.at[tp, step],
                rows_buf.at[tp, step],
                forward_send.at[k, step],
                forward_recv.at[k, step],
                me,
                peer,
            )
            copy.start()
            kept.append(copy)
    for step in range(1, ep):
        to_across[step - 1].wait_recv()
        copy = remote(
            rows_buf.at[across, step],
            rows_buf.at[across, step],
            forward_send.at[2, step],
            forward_recv.at[2, step],
            me,
            beside,
        )
        copy.start()
        to_last.append(copy)
    sends += to_across + to_beside + to_last
    for copy in local[5:]:
        copy.wait()
    for copy in dense_copies + aux_copies + to_beside + to_last:
        copy.wait_recv()

    total = ep * seqs
    gate = up = dense_g = dense_u = None

    def add(total_sum, value):
        return value if total_sum is None else total_sum + value

    for q in range(4):
        rows = rows_buf[q].reshape(total, quarter)
        span = pl.ds(q * quarter, quarter)
        gate = add(gate, jnp.dot(rows, gate_w[span, :], preferred_element_type=f32))
        up = add(up, jnp.dot(rows, up_w[span, :], preferred_element_type=f32))
        dense_g = add(dense_g, lax.dot_general(rows, dgate[q], nt, preferred_element_type=f32))
        dense_u = add(dense_u, lax.dot_general(rows, dup[q], nt, preferred_element_type=f32))
    aux = aux_buf[...].reshape(total, aux_buf.shape[2]).astype(f32)
    aux_lane = lax.broadcasted_iota(jnp.int32, aux.shape, 1)
    weight = jnp.sum(jnp.where(aux_lane == me, aux, 0.0), axis=1, keepdims=True)
    switch = jnp.sum(jnp.where(aux_lane == switch_lane, aux, 0.0), axis=1, keepdims=True)
    hidden = (gate * jax.nn.sigmoid(gate) * up * weight).astype(bf16)
    dense_hidden = (dense_g * jax.nn.sigmoid(dense_g) * dense_u * switch).astype(bf16)

    part_copies = []
    for k, q in enumerate((diagonal, beside, across, tp)):
        value = jnp.dot(hidden, down_w[q], preferred_element_type=f32) + jnp.dot(
            dense_hidden, ddown[q], preferred_element_type=f32
        )
        part_buf[q] = value.astype(bf16).reshape(ep, seqs, quarter)
        if k < 2:
            copy = remote(
                part_buf.at[q], part_peer.at[k], part_send.at[k], part_recv.at[k], me, beside
            )
            copy.start()
            part_copies.append(copy)
    sends += part_copies

    order = list(range(1, ep)) + [0]
    part_copies[0].wait_recv()
    x_copies = {}
    for step in order:
        send_x[step] = (
            part_buf[across, step].astype(f32) + part_peer[0, step].astype(f32)
        ).astype(bf16)
        copy = remote(
            send_x.at[step], recv_x.at[step], x_send.at[step], x_recv.at[step], me, across
        )
        copy.start()
        x_copies[step] = copy
        sends.append(copy)
    part_copies[1].wait_recv()
    combined = None
    ep_copies = []
    for step in order:
        x_copies[step].wait_recv()
        value = (
            part_buf[tp, step].astype(f32)
            + part_peer[1, step].astype(f32)
            + recv_x[step].astype(f32)
        )
        if step == 0:
            combined = value
            continue
        send_ep[step] = value.astype(bf16)
        copy = remote(
            send_ep.at[step],
            recv_ep.at[step],
            ep_send.at[step],
            ep_recv.at[step],
            ep_at(-step),
            tp,
        )
        copy.start()
        ep_copies.append(copy)
    sends += ep_copies
    for step in range(1, ep):
        ep_copies[step - 1].wait_recv()
        combined = combined + recv_ep[step].astype(f32)

    square = jnp.sum(combined * combined, axis=1, keepdims=True)
    square_own[...] = jnp.broadcast_to(square, square_own.shape)
    square_copies = []
    for k, peer in enumerate(near):
        copy = remote(
            square_own, square_peer.at[k], square_send.at[k], square_recv.at[k], me, peer
        )
        copy.start()
        square_copies.append(copy)
    sends += square_copies
    for copy in square_copies:
        copy.wait_recv()
    everything = (square_own[...] + square_peer[0]) + (square_peer[1] + square_peer[2])
    scale = lax.rsqrt(everything[:, 0:1] / width + norm_eps)
    own_stream = stream_buf[tp].astype(f32)
    out_ref[...] = (own_stream + combined * scale * row(out_gain_ref)).astype(bf16)
    state_out.wait()
    for copy in sends:
        copy.wait_send()


def fused_layer(
    resid,
    mix_gain,
    proj_x,
    proj_z,
    proj_b,
    proj_c,
    proj_step,
    step_bias,
    decay_rate,
    conv_taps,
    conv_state,
    scan_state,
    inner_gain,
    proj_out,
    post_gain,
    ffn_gain,
    group_router,
    expert_router,
    route_experts,
    expert_gate,
    expert_up,
    expert_down,
    dense_switch,
    dense_gate,
    dense_up,
    dense_down,
    out_gain,
):
    ep = lax.axis_size("ep")
    seqs, width = resid.shape
    quarter = width // 4
    channels = conv_state.shape[3]
    expert_count = expert_router.shape[1]
    group_count = group_router.shape[1]
    lanes = 128
    hidden_here = expert_gate.shape[2]
    share = dense_gate.shape[0] // 4
    bf16 = jnp.bfloat16
    vmem = pl.BlockSpec(memory_space=pltpu.VMEM)
    hbm = pl.BlockSpec(memory_space=pl.ANY)
    dma = pltpu.SemaphoreType.DMA
    kernel = functools.partial(
        fused_kernel, ep, expert_count // group_count, group_count, expert_count
    )
    smem = pl.BlockSpec(memory_space=pltpu.SMEM)
    earlier = conv_state.transpose(1, 2, 0, 3)
    state = scan_state.reshape(seqs, channels, scan_state.shape[3])
    layer_out, new_state, new_conv = pl.pallas_call(
        kernel,
        out_shape=(
            jax.ShapeDtypeStruct((seqs, quarter), bf16),
            jax.ShapeDtypeStruct(state.shape, state.dtype),
            jax.ShapeDtypeStruct(earlier.shape, earlier.dtype),
        ),
        in_specs=[vmem] * 14 + [smem] * 2 + [hbm] * 11,
        out_specs=(vmem, hbm, vmem),
        scratch_shapes=[
            pltpu.VMEM((4,) + proj_x.shape, bf16),
            pltpu.VMEM(state.shape, state.dtype),
            pltpu.VMEM(state.shape, state.dtype),
            pltpu.VMEM((lanes, width), jnp.float32),
            pltpu.VMEM((width, hidden_here), bf16),
            pltpu.VMEM((width, hidden_here), bf16),
            pltpu.VMEM((4, hidden_here, quarter), bf16),
            pltpu.VMEM((4, share, quarter), bf16),
            pltpu.VMEM((4, share, quarter), bf16),
            pltpu.VMEM((4, share, quarter), bf16),
            pltpu.VMEM((4, seqs, quarter), bf16),
            pltpu.VMEM((seqs, width), bf16),
            pltpu.VMEM((seqs, width), bf16),
            pltpu.VMEM((2, seqs, width // 2), bf16),
            pltpu.VMEM((2, seqs, width // 2), bf16),
            pltpu.VMEM((4, ep, seqs, quarter), bf16),
            pltpu.VMEM((ep, seqs, lanes), bf16),
            pltpu.VMEM((4, ep, seqs, quarter), bf16),
            pltpu.VMEM((2, ep, seqs, quarter), bf16),
            pltpu.VMEM((ep, seqs, quarter), bf16),
            pltpu.VMEM((ep, seqs, quarter), bf16),
            pltpu.VMEM((ep, seqs, quarter), bf16),
            pltpu.VMEM((ep, seqs, quarter), bf16),
            pltpu.VMEM((seqs, 128), jnp.float32),
            pltpu.VMEM((3, seqs, 128), jnp.float32),
            dma((14,)),
            dma,
            dma((9,)),
            dma((9,)),
            dma((3,)),
            dma((3,)),
            dma((ep,)),
            dma((ep,)),
            dma((ep,)),
            dma((ep,)),
            dma((3, ep)),
            dma((3, ep)),
            dma((2,)),
            dma((2,)),
            dma((ep,)),
            dma((ep,)),
            dma((ep,)),
            dma((ep,)),
            dma((3,)),
            dma((3,)),
        ],
        compiler_params=pltpu.CompilerParams(collective_id=0, has_side_effects=True),
        name="fused_layer",
    )(
        proj_out,
        resid,
        mix_gain,
        post_gain,
        ffn_gain,
        expert_router.T,
        group_router.T,
        dense_switch,
        route_experts.T,
        out_gain,
        inner_gain,
        proj_step.T,
        conv_taps,
        earlier,
        step_bias,
        decay_rate,
        proj_x,
        proj_z,
        proj_b,
        proj_c,
        state,
        expert_gate,
        expert_up,
        expert_down,
        dense_gate,
        dense_up,
        dense_down,
    )
    return layer_out, new_state.reshape(scan_state.shape), new_conv.transpose(2, 0, 1, 3)


def on_device(
    resid,
    mix_gain,
    proj_x,
    proj_z,
    proj_b,
    proj_c,
    proj_step,
    step_bias,
    decay_rate,
    conv_taps,
    conv_state,
    scan_state,
    inner_gain,
    proj_out,
    post_gain,
    ffn_gain,
    group_router,
    expert_router,
    route_experts,
    expert_gate,
    expert_up,
    expert_down,
    dense_switch,
    dense_gate,
    dense_up,
    dense_down,
    out_gain,
):
    tp_index = lax.axis_index("tp")
    seqs = resid.shape[0]
    width = resid.shape[1]
    quarter = width // lax.axis_size("tp")
    heads_here = scan_state.shape[1]
    head_dim = scan_state.shape[2]
    state_dim = scan_state.shape[3]
    channels = conv_state.shape[3]
    repeat = heads_here // (channels // state_dim)
    whole_blocks = 2 * seqs * route_experts.shape[1] // expert_router.shape[1] >= seqs
    one_group = channels == state_dim == 128 and expert_router.shape[1] <= 64
    few = lax.axis_size("tp") == 4 and expert_gate.shape[0] == 1
    if whole_blocks and one_group and few:
        return fused_layer(
            resid,
            mix_gain,
            proj_x,
            proj_z,
            proj_b,
            proj_c,
            proj_step,
            step_bias,
            decay_rate,
            conv_taps,
            conv_state,
            scan_state,
            inner_gain,
            proj_out,
            post_gain,
            ffn_gain,
            group_router,
            expert_router,
            route_experts,
            expert_gate,
            expert_up,
            expert_down,
            dense_switch,
            dense_gate,
            dense_up,
            dense_down,
            out_gain,
        )
    normed = scaled_rows(resid, mix_gain).astype(jnp.bfloat16)
    fresh = jnp.stack(
        [
            jnp.dot(normed, proj_x, preferred_element_type=jnp.float32),
            jnp.dot(normed, proj_b, preferred_element_type=jnp.float32),
            jnp.dot(normed, proj_c, preferred_element_type=jnp.float32),
        ],
        axis=1,
    ).astype(jnp.bfloat16)
    gate_z = jnp.dot(normed, proj_z, preferred_element_type=jnp.float32)
    step_all = jnp.dot(normed, proj_step, preferred_element_type=jnp.float32)
    step_raw = lax.dynamic_slice_in_dim(step_all, tp_index * heads_here, heads_here, 1)
    history = jnp.concatenate([conv_state, fresh[:, :, None, :]], axis=2)
    activated = jax.nn.silu(
        jnp.sum(history.astype(jnp.float32) * conv_taps.astype(jnp.float32)[None], axis=2)
    )
    xs_heads = activated[:, 0].reshape(seqs, heads_here, head_dim)
    b_heads = jnp.repeat(activated[:, 1].reshape(seqs, -1, state_dim), repeat, axis=1)
    c_heads = jnp.repeat(activated[:, 2].reshape(seqs, -1, state_dim), repeat, axis=1)
    step = jax.nn.softplus(step_raw + step_bias)
    keep = jnp.exp(-decay_rate * step)
    driven = step[:, :, None] * xs_heads
    new_state = keep[:, :, None, None] * scan_state + driven[:, :, :, None] * b_heads[:, :, None, :]
    read = jnp.sum(new_state * c_heads[:, :, None, :], axis=3).reshape(seqs, channels)
    gated = (read * jax.nn.silu(gate_z) * inner_gain.astype(jnp.float32)).astype(jnp.bfloat16)
    new_conv = history[:, :, 1:, :]
    mixed = lax.psum(
        jnp.dot(gated, proj_out, preferred_element_type=jnp.float32).astype(jnp.bfloat16), "tp"
    ).astype(jnp.float32)
    stream = (resid.astype(jnp.float32) + scaled_rows(mixed, post_gain)).astype(jnp.bfloat16)
    feed = scaled_rows(stream, ffn_gain).astype(jnp.bfloat16)
    feed_quarter = lax.dynamic_slice_in_dim(feed, tp_index * quarter, quarter, 1)
    expert_count = expert_router.shape[1]
    group_size = expert_count // group_router.shape[1]
    pick_count = route_experts.shape[1]
    group_prob = softmax_plain(jnp.dot(feed, group_router, preferred_element_type=jnp.float32))
    expert_logits = jnp.dot(feed, expert_router, preferred_element_type=jnp.float32)
    matches = route_experts[:, :, None] == jnp.arange(expert_count, dtype=jnp.int32)[None, None, :]
    pick_logits = jnp.sum(jnp.where(matches, expert_logits[:, None, :], 0.0), axis=2)
    chosen_group = route_experts[:, 0] // group_size
    group_ids = jnp.arange(group_router.shape[1], dtype=jnp.int32)
    group_weight = jnp.sum(
        jnp.where(chosen_group[:, None] == group_ids[None, :], group_prob, 0.0), axis=1
    )
    pick_weight = softmax_plain(pick_logits) * group_weight[:, None]
    capacity = 2 * seqs * pick_count // expert_count
    flat_picks = route_experts.reshape(-1)
    one_hot = (flat_picks[:, None] == jnp.arange(expert_count, dtype=jnp.int32)[None, :]).astype(
        jnp.int32
    )
    slot = jnp.sum((jnp.cumsum(one_hot, axis=0) - one_hot) * one_hot, axis=1)
    target = flat_picks * capacity + slot
    repeated = jnp.repeat(feed, pick_count, axis=0)
    outgoing = jnp.zeros((expert_count * capacity, width), jnp.bfloat16).at[target].set(repeated)
    outgoing = outgoing.reshape(expert_count, capacity, width)
    arrived = lax.all_to_all(outgoing, "ep", split_axis=0, concat_axis=0, tiled=True)
    sources = arrived.shape[0]
    items = arrived.shape[1]
    rows = arrived.reshape(sources * items, width)
    gate_value = jnp.dot(rows, expert_gate[0], preferred_element_type=jnp.float32)
    up_value = jnp.dot(rows, expert_up[0], preferred_element_type=jnp.float32)
    hidden = (jax.nn.silu(gate_value) * up_value).astype(jnp.bfloat16)
    result = jnp.dot(hidden, expert_down[0], preferred_element_type=jnp.float32).reshape(
        sources, items, width
    )
    summed = lax.psum_scatter(result.astype(jnp.bfloat16), "tp", scatter_dimension=2, tiled=True)
    returned = lax.all_to_all(summed, "ep", split_axis=0, concat_axis=0, tiled=True)
    fetched = returned.reshape(expert_count * capacity, quarter)[target].reshape(
        seqs, pick_count, quarter
    )
    routed = jnp.sum(fetched.astype(jnp.float32) * pick_weight[:, :, None], axis=1)
    gate_piece = jnp.einsum(
        "sd,cd->sc",
        feed_quarter,
        lax.all_gather(dense_gate, "ep", axis=0, tiled=True),
        preferred_element_type=jnp.float32,
    )
    up_piece = jnp.einsum(
        "sd,cd->sc",
        feed_quarter,
        lax.all_gather(dense_up, "ep", axis=0, tiled=True),
        preferred_element_type=jnp.float32,
    )
    gate_sum = gate_piece
    up_sum = up_piece
    gate_sum, up_sum = (
        lax.psum(gate_sum.astype(jnp.bfloat16), "tp").astype(jnp.float32),
        lax.psum(up_sum.astype(jnp.bfloat16), "tp").astype(jnp.float32),
    )
    dense_hidden = (jax.nn.silu(gate_sum) * up_sum).astype(jnp.bfloat16)
    dense_out = jnp.dot(
        dense_hidden,
        lax.all_gather(dense_down, "ep", axis=0, tiled=True),
        preferred_element_type=jnp.float32,
    )
    switch = jax.nn.sigmoid(jnp.dot(feed, dense_switch, preferred_element_type=jnp.float32))
    combined = routed + switch[:, None] * dense_out
    total_square = lax.psum(jnp.sum(combined * combined, axis=1), "tp")
    scale = lax.rsqrt(total_square / width + norm_eps)
    stream_part = lax.dynamic_slice_in_dim(stream, tp_index * quarter, quarter, 1).astype(
        jnp.float32
    )
    layer_out = (stream_part + combined * scale[:, None] * out_gain.astype(jnp.float32)).astype(
        jnp.bfloat16
    )
    return (layer_out, new_state, new_conv)


def solution(mesh):
    placed = (
        P("ep", None),
        P(),
        P(None, "tp"),
        P(None, "tp"),
        P(None, "tp"),
        P(None, "tp"),
        P(),
        P("tp"),
        P("tp"),
        P(None, None, "tp"),
        P("ep", None, None, "tp"),
        P("ep", "tp", None, None),
        P("tp"),
        P("tp", None),
        P(),
        P(),
        P(),
        P(),
        P("ep", None),
        P("ep", None, "tp"),
        P("ep", None, "tp"),
        P("ep", "tp", None),
        P(),
        P("ep", "tp"),
        P("ep", "tp"),
        P("ep", "tp"),
        P("tp"),
    )
    return jax.shard_map(
        on_device,
        mesh=mesh,
        in_specs=placed,
        out_specs=(P("ep", "tp"), P("ep", "tp", None, None), P("ep", None, None, "tp")),
        check_vma=False,
    )
```

profile of v0, /device:TPU:0, one launch (start us, length us, event | category | flops | bytes accessed | tf_op | source)
XLA Modules:
  0.0 58.6 jit_solution(13465953809454468820)
XLA Ops:
  0.6 52.7 %fused_layer.1 = (bf16[32,512]{1,0:T(8,128)(2,1)}, f32[32,128,128]{2,1,0:T(8,128)}, bf16[3,3,32,128]{3,2,1,0:T(8,128)(2,1)}) custom-call(bf16[128,2048]{1,0:T(8,128)(2,1)} %proj_out_ref.1, bf16[32,2048]{1,0:T(8,128)(2,1)} %resid_ref.1, bf16[2048]{0:T(1024)(128)(2,1)} %mix_ref.1, bf16[2048]{0:T(1024)(128)(2,1)} %post_ref.1, bf16[2048]{0:T(1024)(128)(2,1)} %ffn_ref.1, ...), custom_call_target="tpu_custom_call" | custom-call | tf_op jit(solution)/shard_map/fused_layer/pallas_call | solution.py:515
  53.4 1.4 %copy.33 = bf16[32,512]{1,0:T(8,128)(2,1)} copy(bf16[32,512]{1,0:T(8,128)(2,1)} %get-tuple-element.12) | data formatting | bytes 65536
  54.7 0.0 copy-start
  54.7 3.2 %copy.34 = f32[32,2,64,128]{3,2,1,0:T(8,128)} copy(f32[32,2,64,128]{3,2,1,0:T(8,128)} %bitcast.9) | data formatting | bytes 4194304
  57.9 0.0 copy-done
  57.9 0.6 %copy.35 = bf16[32,3,3,128]{3,0,2,1:T(8,128)(2,1)} copy(bf16[32,3,3,128]{3,0,2,1:T(8,128)(2,1)S(1)} %bitcast.11) | data formatting | bytes 147456
Async XLA Ops:
  54.7 3.2 %copy-start = (bf16[3,3,32,128]{3,2,1,0:T(8,128)(2,1)S(1)}, bf16[3,3,32,128]{3,2,1,0:T(8,128)(2,1)}, u32[]{:S(2)}) copy-start(bf16[3,3,32,128]{3,2,1,0:T(8,128)(2,1)} %get-tuple-element.8) | copy-start | bytes 221188
where the time goes:
time: 58.8 us; the launch traced here: 58.6 us
  Pallas kernels  52.7 us (90%)
  local copies, waits for them, and re-layouts  5.2 us (9%)
  between operations  0.65 us (1%)
    pallas_call x1, Pallas kernels, fused_layer(): pl.pallas_call(kernel, out_shape=(jax.ShapeDtypeStruct((seqs, quarter), b...  52.7 us
    unnamed x5, local copies, waits for them, and re-layouts  5.2 us

commit v1 on v0

--- a/solution.py
+++ b/solution.py
@@ -91,8 +91,6 @@
     rows_recv,
     aux_send,
     aux_recv,
-    forward_send,
-    forward_recv,
     part_send,
     part_recv,
     x_send,
@@ -101,6 +99,9 @@
     ep_recv,
     square_send,
     square_recv,
+    entered,
+    z_send,
+    z_aux_send,
 ):
     f32, bf16 = jnp.float32, jnp.bfloat16
     me = lax.axis_index("ep")
@@ -148,9 +149,13 @@
 
     barrier = pltpu.get_barrier_semaphore()
     for step in range(1, ep):
-        pl.semaphore_signal(
-            barrier, inc=1, device_id=(ep_at(step), tp), device_id_type=pl.DeviceIdType.MESH
-        )
+
+        @pl.when(me + step < ep)
+        def _():
+            pl.semaphore_signal(
+                barrier, inc=1, device_id=(ep_at(step), tp), device_id_type=pl.DeviceIdType.MESH
+            )
+
     for peer in near:
         pl.semaphore_signal(
             barrier, inc=1, device_id=(me, peer), device_id_type=pl.DeviceIdType.MESH
@@ -170,11 +175,21 @@
     router_buf[switch_lane : switch_lane + 1, :] = row(switch_ref)
     nt = (((1,), (1,)), ((), ()))
     step_all = lax.dot_general(normed, proj_step_ref[...], nt, preferred_element_type=f32)
-    pl.semaphore_wait(barrier, ep - 1 + 3)
+    pl.semaphore_wait(barrier, me + 3)
+    for step in range(1, ep):
+
+        @pl.when(me >= step)
+        def _():
+            pl.semaphore_signal(
+                entered, inc=1, device_id=(me - step, tp), device_id_type=pl.DeviceIdType.MESH
+            )
+
 
     sends = []
     dense_copies = []
-    for t, (src, dst) in enumerate(dense_pairs):
+
+    def send_dense(t):
+        src, dst = dense_pairs[t]
         for k, peer in enumerate(near):
             copy = remote(
                 src.at[pl.ds(peer * share, share), :],
@@ -186,7 +201,9 @@
             )
             copy.start()
             dense_copies.append(copy)
-    sends += dense_copies
+
+    send_dense(0)
+    send_dense(1)
 
     channels = conv_ref.shape[3]
     heads = bias_ref.shape[0]
@@ -247,24 +264,22 @@
     chip_sum = (mix_own[...].astype(f32) + mix_peer[...].astype(f32)).astype(bf16)
     half_own[0] = chip_sum[:, :half]
     half_own[1] = chip_sum[:, half:]
-    halves = []
-    for k, peer in enumerate((across, diagonal)):
-        copy = remote(
-            half_own.at[core],
-            half_far.at[core],
-            mix_send.at[1 + k],
-            mix_recv.at[1 + k],
-            me,
-            peer,
-        )
-        copy.start()
-        halves.append(copy)
-    sends += halves
+    over_x = remote(
+        half_own.at[core], half_far.at[core], mix_send.at[1], mix_recv.at[1], me, across
+    )
+    over_x.start()
+    send_dense(2)
+    sends += dense_copies
 
     state_out = pltpu.make_async_copy(new_state_buf, new_state_hbm, state_sem)
     state_out.start()
-    for copy in halves:
-        copy.wait_recv()
+    over_x.wait_recv()
+    to_core = remote(
+        half_far.at[core], half_far.at[core], mix_send.at[2], mix_recv.at[2], me, beside
+    )
+    to_core.start()
+    sends += [over_x, to_core]
+    to_core.wait_recv()
 
     far_sum = jnp.concatenate([half_far[0], half_far[1]], axis=1)
     mixed = chip_sum.astype(f32) + far_sum.astype(f32)
@@ -274,24 +289,71 @@
     ).astype(bf16)
     stream_f = stream.astype(f32)
     feed_scale = lax.rsqrt(jnp.mean(stream_f * stream_f, axis=1, keepdims=True) + norm_eps)
-    feed = (stream_f * feed_scale * row(ffn_ref)).astype(bf16)
+    feed_f = stream_f * feed_scale * row(ffn_ref)
+    feed = feed_f.astype(bf16)
+    my_z, my_y = me // 2, me % 2
+    nz = ep // 2
+    here = my_y * nz + my_z
+
+    def feed_of(q):
+        value = feed_f[:, :quarter]
+        for other in range(1, 4):
+            piece = feed_f[:, other * quarter : (other + 1) * quarter]
+            value = jnp.where(q == other, piece, value)
+        return value.astype(bf16)
+
+    quarters = (tp, beside, across, diagonal)
+    for k, q in enumerate(quarters):
+        rows_buf[k, here] = feed_of(q)
     for q in range(4):
-        rows_buf[q, 0] = feed[:, q * quarter : (q + 1) * quarter]
         stream_buf[q] = stream[:, q * quarter : (q + 1) * quarter]
 
-    rows_copies = []
-    for step in range(1, ep):
-        copy = remote(
-            rows_buf.at[tp, 0],
-            rows_buf.at[tp, step],
-            rows_send.at[step],
-            rows_recv.at[step],
-            ep_at(step),
+    @pl.when(me + 1 < ep)
+    def _():
+        pl.semaphore_wait(entered, ep - 1 - me)
+
+    others = [j + (j - my_z + nz) // nz for j in range(nz - 1)]
+
+    def rows_copy(k, at, send, ep_to, tp_to, k_to):
+        return remote(
+            rows_buf.at[k, at],
+            rows_buf.at[k_to, at],
+            rows_send.at[send, at],
+            rows_recv.at[k_to, at],
+            ep_to,
+            tp_to,
+        )
+
+    def aux_copy(at, send, ep_to):
+        return remote(
+            aux_buf.at[at], aux_buf.at[at], aux_send.at[send, at], aux_recv.at[at], ep_to, tp
+        )
+
+    def z_rows(z):
+        return remote(
+            rows_buf.at[0, here],
+            rows_buf.at[0, here],
+            z_send.at[z],
+            rows_recv.at[0, here],
+            z * 2 + my_y,
             tp,
         )
+
+    def z_aux(z):
+        return remote(
+            aux_buf.at[here], aux_buf.at[here], z_aux_send.at[z], aux_recv.at[here],
+            z * 2 + my_y, tp,
+        )
+
+    def started(copy):
         copy.start()
-        rows_copies.append(copy)
-    sends += rows_copies
+        sends.append(copy)
+
+    for z in reversed(others):
+        started(z_rows(z))
+    over_y = my_z * 2 + 1 - my_y
+    started(rows_copy(0, here, 0, over_y, tp, 0))
+    started(rows_copy(2, here, 1, over_y, tp, 2))
 
     logits = lax.dot_general(
         feed, router_buf[...].astype(bf16), nt, preferred_element_type=f32
@@ -320,128 +382,151 @@
         group, axis=1, keepdims=True
     )
     pick = pick / jnp.sum(pick, axis=1, keepdims=True) * group_weight
-    aux_buf[0] = jnp.where(lane == switch_lane, jax.nn.sigmoid(logits), pick).astype(bf16)
-    aux_copies = []
-    for step in range(1, ep):
-        copy = remote(
-            aux_buf.at[0],
-            aux_buf.at[step],
-            aux_send.at[step],
-            aux_recv.at[step],
-            ep_at(step),
-            tp,
-        )
-        copy.start()
-        aux_copies.append(copy)
-    sends += aux_copies
-
-    to_beside, to_across, to_last = [], [], []
-    for step in range(1, ep):
-        rows_copies[step - 1].wait_recv()
-        for k, (peer, kept) in enumerate(((across, to_across), (beside, to_beside))):
-            copy = remote(
-                rows_buf.at[tp, step],
-                rows_buf.at[tp, step],
-                forward_send.at[k, step],
-                forward_recv.at[k, step],
-                me,
-                peer,
-            )
-            copy.start()
-            kept.append(copy)
-    for step in range(1, ep):
-        to_across[step - 1].wait_recv()
-        copy = remote(
-            rows_buf.at[across, step],
-            rows_buf.at[across, step],
-            forward_send.at[2, step],
-            forward_recv.at[2, step],
+    aux_buf[here] = jnp.where(lane == switch_lane, jax.nn.sigmoid(logits), pick).astype(bf16)
+    for z in reversed(others):
+        started(z_aux(z))
+    started(aux_copy(here, 0, over_y))
+
+    total = nz * seqs
+    sides = (my_y, 1 - my_y)
+
+    def at_of(side, z):
+        return sides[side] * nz + z
+
+    def arrived(k, at):
+        rows_copy(k, at, 0, me, beside, k).wait_recv()
+
+    there = at_of(1, my_z)
+    for z in others:
+        at = at_of(0, z)
+        arrived(0, at)
+        started(rows_copy(0, at, 0, over_y, tp, 0))
+        started(rows_copy(0, at, 1, me, across, 2))
+        started(rows_copy(0, at, 2, me, beside, 1))
+    arrived(0, there)
+    started(rows_copy(0, there, 2, me, beside, 1))
+    arrived(2, there)
+    started(rows_copy(2, there, 3, me, beside, 3))
+    for z in others:
+        at = at_of(0, z)
+        aux_copy(at, 0, me).wait_recv()
+        started(aux_copy(at, 0, over_y))
+    for z in others:
+        at = at_of(1, z)
+        arrived(0, at)
+        started(rows_copy(0, at, 1, me, across, 2))
+        started(rows_copy(0, at, 2, me, beside, 1))
+    for z in others:
+        at = at_of(0, z)
+        arrived(2, at)
+        started(rows_copy(2, at, 3, me, beside, 3))
+
+    def gather_end(side):
+        for z in range(nz) if side else others:
+            at = at_of(side, z)
+            if side:
+                aux_copy(at, 0, me).wait_recv()
+            arrived(1, at)
+            arrived(3, at)
+
+    def add(total_sum, value):
+        return value if total_sum is None else total_sum + value
+
+    def part_copy(k, side):
+        block = pl.ds(sides[side] * nz, nz)
+        return remote(
+            part_buf.at[(diagonal, beside)[k], block],
+            part_peer.at[k, block],
+            part_send.at[k, side],
+            part_recv.at[k, side],
             me,
             beside,
         )
-        copy.start()
-        to_last.append(copy)
-    sends += to_across + to_beside + to_last
+
+    def feed_forward(side):
+        block = pl.ds(sides[side] * nz, nz)
+        gate = up = dense_g = dense_u = None
+        for k, q in enumerate(quarters):
+            rows = rows_buf[k, block].reshape(total, quarter)
+            span = pl.ds(pl.multiple_of(q * quarter, quarter), quarter)
+            gate = add(gate, jnp.dot(rows, gate_w[span, :], preferred_element_type=f32))
+            up = add(up, jnp.dot(rows, up_w[span, :], preferred_element_type=f32))
+            dense_g = add(
+                dense_g, lax.dot_general(rows, dgate[q], nt, preferred_element_type=f32)
+            )
+            dense_u = add(dense_u, lax.dot_general(rows, dup[q], nt, preferred_element_type=f32))
+        aux = aux_buf[block].reshape(total, aux_buf.shape[2]).astype(f32)
+        aux_lane = lax.broadcasted_iota(jnp.int32, aux.shape, 1)
+        weight = jnp.sum(jnp.where(aux_lane == me, aux, 0.0), axis=1, keepdims=True)
+        switch = jnp.sum(jnp.where(aux_lane == switch_lane, aux, 0.0), axis=1, keepdims=True)
+        hidden = (gate * jax.nn.sigmoid(gate) * up * weight).astype(bf16)
+        dense_hidden = (dense_g * jax.nn.sigmoid(dense_g) * dense_u * switch).astype(bf16)
+        for k, q in enumerate((diagonal, beside, across, tp)):
+            value = jnp.dot(hidden, down_w[q], preferred_element_type=f32) + jnp.dot(
+                dense_hidden, ddown[q], preferred_element_type=f32
+            )
+            part_buf[q, block] = value.astype(bf16).reshape(nz, seqs, quarter)
+            if k < 2:
+                started(part_copy(k, side))
+
+    def targets(side):
+        return list(range(nz)) if side else others + [my_z]
+
+    def x_copy(at):
+        return remote(send_x.at[at], recv_x.at[at], x_send.at[at], x_recv.at[at], me, across)
+
+    def sums_over_x(side):
+        part_copy(0, side).wait_recv()
+        for z in targets(side):
+            at = at_of(side, z)
+            send_x[at] = (
+                part_buf[across, at].astype(f32) + part_peer[0, at].astype(f32)
+            ).astype(bf16)
+            started(x_copy(at))
+
+    def ep_copy(at, slot, ep_to):
+        return remote(
+            send_ep.at[at], recv_ep.at[slot], ep_send.at[at], ep_recv.at[slot], ep_to, tp
+        )
+
+    def summed(at):
+        x_copy(at).wait_recv()
+        return (
+            part_buf[tp, at].astype(f32)
+            + part_peer[1, at].astype(f32)
+            + recv_x[at].astype(f32)
+        )
+
+    def sums_over_ep(side):
+        part_copy(1, side).wait_recv()
+        for z in range(nz) if side else others:
+            at = at_of(side, z)
+            send_ep[at] = summed(at).astype(bf16)
+            started(ep_copy(at, here, z * 2 + sides[side]))
+
     for copy in local[5:]:
         copy.wait()
-    for copy in dense_copies + aux_copies + to_beside + to_last:
+    for copy in dense_copies:
         copy.wait_recv()
-
-    total = ep * seqs
-    gate = up = dense_g = dense_u = None
-
-    def add(total_sum, value):
-        return value if total_sum is None else total_sum + value
-
-    for q in range(4):
-        rows = rows_buf[q].reshape(total, quarter)
-        span = pl.ds(q * quarter, quarter)
-        gate = add(gate, jnp.dot(rows, gate_w[span, :], preferred_element_type=f32))
-        up = add(up, jnp.dot(rows, up_w[span, :], preferred_element_type=f32))
-        dense_g = add(dense_g, lax.dot_general(rows, dgate[q], nt, preferred_element_type=f32))
-        dense_u = add(dense_u, lax.dot_general(rows, dup[q], nt, preferred_element_type=f32))
-    aux = aux_buf[...].reshape(total, aux_buf.shape[2]).astype(f32)
-    aux_lane = lax.broadcasted_iota(jnp.int32, aux.shape, 1)
-    weight = jnp.sum(jnp.where(aux_lane == me, aux, 0.0), axis=1, keepdims=True)
-    switch = jnp.sum(jnp.where(aux_lane == switch_lane, aux, 0.0), axis=1, keepdims=True)
-    hidden = (gate * jax.nn.sigmoid(gate) * up * weight).astype(bf16)
-    dense_hidden = (dense_g * jax.nn.sigmoid(dense_g) * dense_u * switch).astype(bf16)
-
-    part_copies = []
-    for k, q in enumerate((diagonal, beside, across, tp)):
-        value = jnp.dot(hidden, down_w[q], preferred_element_type=f32) + jnp.dot(
-            dense_hidden, ddown[q], preferred_element_type=f32
-        )
-        part_buf[q] = value.astype(bf16).reshape(ep, seqs, quarter)
-        if k < 2:
-            copy = remote(
-                part_buf.at[q], part_peer.at[k], part_send.at[k], part_recv.at[k], me, beside
-            )
-            copy.start()
-            part_copies.append(copy)
-    sends += part_copies
-
-    order = list(range(1, ep)) + [0]
-    part_copies[0].wait_recv()
-    x_copies = {}
-    for step in order:
-        send_x[step] = (
-            part_buf[across, step].astype(f32) + part_peer[0, step].astype(f32)
-        ).astype(bf16)
-        copy = remote(
-            send_x.at[step], recv_x.at[step], x_send.at[step], x_recv.at[step], me, across
-        )
-        copy.start()
-        x_copies[step] = copy
-        sends.append(copy)
-    part_copies[1].wait_recv()
-    combined = None
-    ep_copies = []
-    for step in order:
-        x_copies[step].wait_recv()
-        value = (
-            part_buf[tp, step].astype(f32)
-            + part_peer[1, step].astype(f32)
-            + recv_x[step].astype(f32)
-        )
-        if step == 0:
-            combined = value
-            continue
-        send_ep[step] = value.astype(bf16)
-        copy = remote(
-            send_ep.at[step],
-            recv_ep.at[step],
-            ep_send.at[step],
-            ep_recv.at[step],
-            ep_at(-step),
-            tp,
-        )
-        copy.start()
-        ep_copies.append(copy)
-    sends += ep_copies
-    for step in range(1, ep):
-        ep_copies[step - 1].wait_recv()
-        combined = combined + recv_ep[step].astype(f32)
+    gather_end(0)
+    feed_forward(0)
+    for z in others:
+        at = at_of(1, z)
+        arrived(2, at)
+        started(rows_copy(2, at, 3, me, beside, 3))
+    sums_over_x(0)
+    gather_end(1)
+    feed_forward(1)
+    sums_over_ep(0)
+    sums_over_x(1)
+    combined = summed(here)
+    sums_over_ep(1)
+
+    for side in range(2):
+        for z in range(nz) if side else others:
+            at = at_of(side, z)
+            ep_copy(at, at, me).wait_recv()
+            combined = combined + recv_ep[at].astype(f32)
 
     square = jnp.sum(combined * combined, axis=1, keepdims=True)
     square_own[...] = jnp.broadcast_to(square, square_own.shape)
@@ -553,20 +638,21 @@
             dma((9,)),
             dma((3,)),
             dma((3,)),
+            dma((4, ep)),
+            dma((4, ep)),
+            dma((1, ep)),
             dma((ep,)),
-            dma((ep,)),
-            dma((ep,)),
-            dma((ep,)),
-            dma((3, ep)),
-            dma((3, ep)),
-            dma((2,)),
-            dma((2,)),
+            dma((2, 2)),
+            dma((2, 2)),
             dma((ep,)),
             dma((ep,)),
             dma((ep,)),
             dma((ep,)),
             dma((3,)),
             dma((3,)),
+            pltpu.SemaphoreType.REGULAR,
+            dma((ep,)),
+            dma((ep,)),
         ],
         compiler_params=pltpu.CompilerParams(collective_id=0, has_side_effects=True),
         name="fused_layer",
@@ -643,6 +729,7 @@
     whole_blocks = 2 * seqs * route_experts.shape[1] // expert_router.shape[1] >= seqs
     one_group = channels == state_dim == 128 and expert_router.shape[1] <= 64
     few = lax.axis_size("tp") == 4 and expert_gate.shape[0] == 1
+    few = few and lax.axis_size("ep") % 2 == 0
     if whole_blocks and one_group and few:
         return fused_layer(
             resid,

time: 58.8 us -> 51.3 us (0.87)
  Pallas kernels: 52.7 us -> 45.3 us
    pallas_call x1, Pallas kernels: 52.7 us -> 45.3 us  [fused_layer(): pl.pallas_call(kernel, out_shape=(jax.ShapeDtypeStruct((seqs, quarter), b...]
where the time goes in v1:
time: 51.3 us; the launch traced here: 51.1 us
  Pallas kernels  45.3 us (88%)
  local copies, waits for them, and re-layouts  5.2 us (10%)
  between operations  0.65 us (1%)
    pallas_call x1, Pallas kernels, fused_layer(): pl.pallas_call(kernel, out_shape=(jax.ShapeDtypeStruct((seqs, quarter), b...  45.3 us
    unnamed x5, local copies, waits for them, and re-layouts  5.2 us

profile of v1, /device:TPU:0, one launch (start us, length us, event | category | flops | bytes accessed | tf_op | source)
XLA Modules:
  0.0 51.1 jit_solution(9946949700878088827)
XLA Ops:
  0.6 45.3 %fused_layer.1 = (bf16[32,512]{1,0:T(8,128)(2,1)}, f32[32,128,128]{2,1,0:T(8,128)}, bf16[3,3,32,128]{3,2,1,0:T(8,128)(2,1)}) custom-call(bf16[128,2048]{1,0:T(8,128)(2,1)} %proj_out_ref.1, bf16[32,2048]{1,0:T(8,128)(2,1)} %resid_ref.1, bf16[2048]{0:T(1024)(128)(2,1)} %mix_ref.1, bf16[2048]{0:T(1024)(128)(2,1)} %post_ref.1, bf16[2048]{0:T(1024)(128)(2,1)} %ffn_ref.1, ...), custom_call_target="tpu_custom_call" | custom-call | tf_op jit(solution)/shard_map/fused_layer/pallas_call | solution.py:600
  45.9 1.4 %copy.33 = bf16[32,512]{1,0:T(8,128)(2,1)} copy(bf16[32,512]{1,0:T(8,128)(2,1)} %get-tuple-element.12) | data formatting | bytes 65536
  47.3 0.0 copy-start
  47.3 3.2 %copy.34 = f32[32,2,64,128]{3,2,1,0:T(8,128)} copy(f32[32,2,64,128]{3,2,1,0:T(8,128)} %bitcast.9) | data formatting | bytes 4194304
  50.5 0.0 copy-done
  50.5 0.6 %copy.35 = bf16[32,3,3,128]{3,0,2,1:T(8,128)(2,1)} copy(bf16[32,3,3,128]{3,0,2,1:T(8,128)(2,1)S(1)} %bitcast.11) | data formatting | bytes 147456
Async XLA Ops:
  47.3 3.2 %copy-start = (bf16[3,3,32,128]{3,2,1,0:T(8,128)(2,1)S(1)}, bf16[3,3,32,128]{3,2,1,0:T(8,128)(2,1)}, u32[]{:S(2)}) copy-start(bf16[3,3,32,128]{3,2,1,0:T(8,128)(2,1)} %get-tuple-element.8) | copy-start | bytes 221188

commit v2 on v1

--- a/solution.py
+++ b/solution.py
@@ -54,11 +54,10 @@
     dense_up_hbm,
     dense_down_hbm,
     out_ref,
-    new_state_hbm,
+    new_state_ref,
     new_conv_ref,
     proj_w,
     state_buf,
-    new_state_buf,
     router_buf,
     gate_w,
     up_w,
@@ -82,7 +81,6 @@
     square_own,
     square_peer,
     local_sem,
-    state_sem,
     dense_send,
     dense_recv,
     mix_send,
@@ -249,7 +247,7 @@
             columns[:, t : t + 1] * state_buf[t]
             + columns[:, seqs + t : seqs + t + 1] * vec_in[t : t + 1]
         )
-        new_state_buf[t] = fresh_state
+        new_state_ref[t] = fresh_state
         value = jnp.sum(fresh_state * vec_read[t : t + 1], axis=1, keepdims=True)
         read = jnp.where(read_lane == t, value, read)
     read = read.T[0:seqs]
@@ -271,8 +269,6 @@
     send_dense(2)
     sends += dense_copies
 
-    state_out = pltpu.make_async_copy(new_state_buf, new_state_hbm, state_sem)
-    state_out.start()
     over_x.wait_recv()
     to_core = remote(
         half_far.at[core], half_far.at[core], mix_send.at[2], mix_recv.at[2], me, beside
@@ -312,7 +308,12 @@
     def _():
         pl.semaphore_wait(entered, ep - 1 - me)
 
-    others = [j + (j - my_z + nz) // nz for j in range(nz - 1)]
+    def other(j):
+        return j + (j - my_z + nz) // nz
+
+    others = [other(j) for j in range(nz - 1)]
+    upper = my_z // (nz // 2)
+    far_first = [other(upper * j + (1 - upper) * (nz - 2 - j)) for j in range(nz - 1)]
 
     def rows_copy(k, at, send, ep_to, tp_to, k_to):
         return remote(
@@ -349,7 +350,7 @@
         copy.start()
         sends.append(copy)
 
-    for z in reversed(others):
+    for z in far_first:
         started(z_rows(z))
     over_y = my_z * 2 + 1 - my_y
     started(rows_copy(0, here, 0, over_y, tp, 0))
@@ -383,7 +384,7 @@
     )
     pick = pick / jnp.sum(pick, axis=1, keepdims=True) * group_weight
     aux_buf[here] = jnp.where(lane == switch_lane, jax.nn.sigmoid(logits), pick).astype(bf16)
-    for z in reversed(others):
+    for z in far_first:
         started(z_aux(z))
     started(aux_copy(here, 0, over_y))
 
@@ -469,15 +470,14 @@
             if k < 2:
                 started(part_copy(k, side))
 
-    def targets(side):
-        return list(range(nz)) if side else others + [my_z]
+    far_then_own = far_first + [my_z]
 
     def x_copy(at):
         return remote(send_x.at[at], recv_x.at[at], x_send.at[at], x_recv.at[at], me, across)
 
     def sums_over_x(side):
         part_copy(0, side).wait_recv()
-        for z in targets(side):
+        for z in far_then_own:
             at = at_of(side, z)
             send_x[at] = (
                 part_buf[across, at].astype(f32) + part_peer[0, at].astype(f32)
@@ -499,7 +499,7 @@
 
     def sums_over_ep(side):
         part_copy(1, side).wait_recv()
-        for z in range(nz) if side else others:
+        for z in far_then_own if side else far_first:
             at = at_of(side, z)
             send_ep[at] = summed(at).astype(bf16)
             started(ep_copy(at, here, z * 2 + sides[side]))
@@ -529,7 +529,11 @@
             combined = combined + recv_ep[at].astype(f32)
 
     square = jnp.sum(combined * combined, axis=1, keepdims=True)
-    square_own[...] = jnp.broadcast_to(square, square_own.shape)
+    lanes = square_own.shape[1]
+    row_id = lax.broadcasted_iota(jnp.int32, (seqs, lanes), 0)
+    diagonal_lane = row_id == lax.broadcasted_iota(jnp.int32, (seqs, lanes), 1)
+    square_row = jnp.sum(jnp.where(diagonal_lane, square, 0.0), axis=0, keepdims=True)
+    square_own[...] = jnp.broadcast_to(square_row, square_own.shape)
     square_copies = []
     for k, peer in enumerate(near):
         copy = remote(
@@ -541,12 +545,21 @@
     for copy in square_copies:
         copy.wait_recv()
     everything = (square_own[...] + square_peer[0]) + (square_peer[1] + square_peer[2])
-    scale = lax.rsqrt(everything[:, 0:1] / width + norm_eps)
+    spread = jnp.where(diagonal_lane, everything[0:1], 0.0)
+    scale = lax.rsqrt(jnp.sum(spread, axis=1, keepdims=True) / width + norm_eps)
     own_stream = stream_buf[tp].astype(f32)
     out_ref[...] = (own_stream + combined * scale * row(out_gain_ref)).astype(bf16)
-    state_out.wait()
     for copy in sends:
         copy.wait_send()
+
+
+def write_kernel(out_ref, state_ref, conv_ref, out_hbm, state_hbm, conv_hbm, sems):
+    pairs = ((state_ref, state_hbm), (conv_ref, conv_hbm), (out_ref, out_hbm))
+    copies = [pltpu.make_async_copy(src, dst, sems.at[k]) for k, (src, dst) in enumerate(pairs)]
+    for copy in copies:
+        copy.start()
+    for copy in copies:
+        copy.wait()
 
 
 def fused_layer(
@@ -597,18 +610,17 @@
     smem = pl.BlockSpec(memory_space=pltpu.SMEM)
     earlier = conv_state.transpose(1, 2, 0, 3)
     state = scan_state.reshape(seqs, channels, scan_state.shape[3])
-    layer_out, new_state, new_conv = pl.pallas_call(
+    results = pl.pallas_call(
         kernel,
         out_shape=(
-            jax.ShapeDtypeStruct((seqs, quarter), bf16),
-            jax.ShapeDtypeStruct(state.shape, state.dtype),
-            jax.ShapeDtypeStruct(earlier.shape, earlier.dtype),
+            pltpu.VMEM((seqs, quarter), bf16),
+            pltpu.VMEM(state.shape, state.dtype),
+            pltpu.VMEM(earlier.shape, earlier.dtype),
         ),
         in_specs=[vmem] * 14 + [smem] * 2 + [hbm] * 11,
-        out_specs=(vmem, hbm, vmem),
+        out_specs=(vmem, vmem, vmem),
         scratch_shapes=[
             pltpu.VMEM((4,) + proj_x.shape, bf16),
-            pltpu.VMEM(state.shape, state.dtype),
             pltpu.VMEM(state.shape, state.dtype),
             pltpu.VMEM((lanes, width), jnp.float32),
             pltpu.VMEM((width, hidden_here), bf16),
@@ -630,10 +642,9 @@
             pltpu.VMEM((ep, seqs, quarter), bf16),
             pltpu.VMEM((ep, seqs, quarter), bf16),
             pltpu.VMEM((ep, seqs, quarter), bf16),
-            pltpu.VMEM((seqs, 128), jnp.float32),
-            pltpu.VMEM((3, seqs, 128), jnp.float32),
+            pltpu.VMEM((8, lanes), jnp.float32),
+            pltpu.VMEM((3, 8, lanes), jnp.float32),
             dma((14,)),
-            dma,
             dma((9,)),
             dma((9,)),
             dma((3,)),
@@ -685,6 +696,15 @@
         dense_up,
         dense_down,
     )
+    layer_out, new_state, new_conv = pl.pallas_call(
+        write_kernel,
+        out_shape=tuple(jax.ShapeDtypeStruct(one.shape, one.dtype) for one in results),
+        in_specs=[vmem] * 3,
+        out_specs=(hbm, hbm, hbm),
+        scratch_shapes=[dma((3,))],
+        compiler_params=pltpu.CompilerParams(vmem_limit_bytes=4 << 20),
+        name="write_results",
+    )(*results)
     return layer_out, new_state.reshape(scan_state.shape), new_conv.transpose(2, 0, 1, 3)
 
 

time: 51.3 us -> 47 us (0.916)
  local copies, waits for them, and re-layouts: 5.2 us -> 0 us
  Pallas kernels: 45.3 us -> 46.2 us
    unnamed x5 -> x0, local copies, waits for them, and re-layouts: 5.2 us -> none
    pallas_call x1 -> x2, Pallas kernels: 45.3 us -> 46.2 us  [the longest x1 44.9 us: fused_layer(): pl.pallas_call(kernel, out_shape=(pltpu.VMEM((seqs, quarter), bf16), pltp...]
where the time goes in v2:
time: 47 us; the launch traced here: 46.9 us
  Pallas kernels  46.2 us (98%)
  between operations  0.65 us (1%)
    pallas_call x1, Pallas kernels, fused_layer(): pl.pallas_call(kernel, out_shape=(pltpu.VMEM((seqs, quarter), bf16), pltp...  44.9 us
    pallas_call x1, Pallas kernels, fused_layer(): pl.pallas_call(write_kernel, out_shape=tuple((jax.ShapeDtypeStruct(one.sh...  1.36 us

profile of v2, /device:TPU:0, one launch (start us, length us, event | category | flops | bytes accessed | tf_op | source)
XLA Modules:
  0.0 46.9 jit_solution(5696146775543517006)
XLA Ops:
  0.6 44.9 %fused_layer.1 = (bf16[32,512]{1,0:T(8,128)(2,1)S(1)}, f32[32,128,128]{2,1,0:T(8,128)S(1)}, bf16[3,3,32,128]{3,2,1,0:T(8,128)(2,1)S(1)}) custom-call(bf16[128,2048]{1,0:T(8,128)(2,1)} %proj_out_ref.1, bf16[32,2048]{1,0:T(8,128)(2,1)} %resid_ref.1, bf16[2048]{0:T(1024)(128)(2,1)} %mix_ref.1, bf16[2048]{0:T(1024)(128)(2,1)} %post_ref.1, ...), custom_call_target="tpu_custom_call" | custom-call | tf_op jit(solution)/shard_map/fused_layer/pallas_call | solution.py:613
  45.5 1.4 %write_results.1 = (bf16[32,512]{1,0:T(8,128)(2,1)}, f32[32,128,128]{2,1,0:T(8,128)}, bf16[3,3,32,128]{3,2,1,0:T(8,128)(2,1)}) custom-call(bf16[32,512]{1,0:T(8,128)(2,1)S(1)} %get-tuple-element.9.out_ref, f32[32,128,128]{2,1,0:T(8,128)S(1)} %get-tuple-element.10.state_ref, bf16[3,3,32,128]{3,2,1,0:T(8,128)(2,1)S(1)} %get-tuple-element.11.conv_ref), custom_call_target="tpu_custom_call" | custom-call | tf_op jit(solution)/shard_map/write_results/pallas_call | solution.py:699

commit v3 on v2

--- a/solution.py
+++ b/solution.py
@@ -58,13 +58,13 @@
     new_conv_ref,
     proj_w,
     state_buf,
+    keep_rows,
+    vec_in_rows,
     router_buf,
     gate_w,
     up_w,
     down_w,
-    dgate,
-    dup,
-    ddown,
+    dense_w,
     stream_buf,
     mix_own,
     mix_peer,
@@ -98,8 +98,7 @@
     square_send,
     square_recv,
     entered,
-    z_send,
-    z_aux_send,
+    side_recv,
 ):
     f32, bf16 = jnp.float32, jnp.bfloat16
     me = lax.axis_index("ep")
@@ -112,7 +111,8 @@
     near = (beside, across, diagonal)
     seqs, width = resid_ref.shape
     quarter = width // 4
-    share = dgate.shape[1]
+    share = dense_w.shape[2]
+    dgate, dup, ddown = dense_w.at[0], dense_w.at[1], dense_w.at[2]
 
     def remote(src, dst, send, recv, ep_to, tp_to):
         return pltpu.make_async_remote_copy(
@@ -127,23 +127,22 @@
     def ep_at(step):
         return lax.rem(me + step + ep, ep)
 
-    local = []
-
-    def load(src, dst):
-        copy = pltpu.make_async_copy(src, dst, local_sem.at[len(local)])
-        copy.start()
-        local.append(copy)
+    def load(src, dst, at):
+        pltpu.make_async_copy(src, dst, local_sem.at[at]).start()
+
+    def loaded(dst, at):
+        pltpu.make_async_copy(dst, dst, local_sem.at[at]).wait()
 
     for k, src in enumerate((proj_x_hbm, proj_b_hbm, proj_c_hbm, proj_z_hbm)):
-        load(src, proj_w.at[k])
-    load(state_hbm, state_buf)
-    load(gate_hbm.at[0], gate_w)
-    load(up_hbm.at[0], up_w)
+        load(src, proj_w.at[k], k)
+    load(state_hbm, state_buf, 4)
+    load(gate_hbm.at[0], gate_w, 5)
+    load(up_hbm.at[0], up_w, 6)
     for q in range(4):
-        load(down_hbm.at[0, :, pl.ds(q * quarter, quarter)], down_w.at[q])
+        load(down_hbm.at[0, :, pl.ds(q * quarter, quarter)], down_w.at[q], 7)
     dense_pairs = ((dense_gate_hbm, dgate), (dense_up_hbm, dup), (dense_down_hbm, ddown))
     for src, dst in dense_pairs:
-        load(src.at[pl.ds(tp * share, share), :], dst.at[tp])
+        load(src.at[pl.ds(tp * share, share), :], dst.at[tp], 8)
 
     barrier = pltpu.get_barrier_semaphore()
     for step in range(1, ep):
@@ -184,24 +183,20 @@
 
 
     sends = []
-    dense_copies = []
 
     def send_dense(t):
         src, dst = dense_pairs[t]
-        for k, peer in enumerate(near):
-            copy = remote(
+        for peer in near:
+            remote(
                 src.at[pl.ds(peer * share, share), :],
                 dst.at[tp],
-                dense_send.at[3 * t + k],
-                dense_recv.at[3 * t + k],
+                dense_send,
+                dense_recv,
                 me,
                 peer,
-            )
-            copy.start()
-            dense_copies.append(copy)
+            ).start()
 
     send_dense(0)
-    send_dense(1)
 
     channels = conv_ref.shape[3]
     heads = bias_ref.shape[0]
@@ -210,7 +205,7 @@
     old = conv_ref.shape[1]
     active = []
     for k in range(3):
-        local[k].wait()
+        loaded(proj_w.at[k], k)
         fresh = jnp.dot(normed, proj_w[k], preferred_element_type=f32).astype(bf16)
         summed = conv_ref[k, 0].astype(f32) * taps[k, 0:1]
         for tap in range(1, old):
@@ -221,11 +216,10 @@
         summed = summed + fresh.astype(f32) * taps[k, old : old + 1]
         active.append(summed * jax.nn.sigmoid(summed))
     inputs, vec_in, vec_read = active
-    local[3].wait()
+    loaded(proj_w.at[3], 3)
     gate_z = jnp.dot(normed, proj_w[3], preferred_element_type=f32)
     step_lane = lax.broadcasted_iota(jnp.int32, step_all.shape, 1)
     lane_in = lax.broadcasted_iota(jnp.int32, (seqs, channels), 1)
-    keep = jnp.zeros((seqs, channels), f32)
     stepped = jnp.zeros((seqs, channels), f32)
     for h in range(heads):
         raw = jnp.sum(
@@ -234,22 +228,31 @@
         raw = raw + bias_ref[h]
         step = jnp.maximum(raw, 0.0) + jnp.log1p(jnp.exp(-jnp.abs(raw)))
         mine = (lane_in >= h * head_dim) & (lane_in < (h + 1) * head_dim)
-        keep = jnp.where(mine, jnp.exp(-decay_ref[h] * step), keep)
+        keep_rows[h] = jnp.broadcast_to(jnp.exp(-decay_ref[h] * step), (seqs, channels))
         stepped = jnp.where(mine, step, stepped)
     columns = jnp.concatenate(
-        [keep, stepped * inputs, jnp.zeros((channels - 2 * seqs, channels), f32)], axis=0
+        [stepped * inputs, jnp.zeros((channels - seqs, channels), f32)], axis=0
     ).T
-    local[4].wait()
-    read_lane = lax.broadcasted_iota(jnp.int32, (channels, channels), 1)
-    read = jnp.zeros((channels, channels), f32)
+    vec_in_rows[...] = vec_in
+    read_rows = vec_read.astype(bf16)
+    loaded(state_buf, 4)
+    read_lane = lax.broadcasted_iota(jnp.int32, (head_dim, seqs), 1)
+    reads = [jnp.zeros((head_dim, seqs), f32) for h in range(heads)]
     for t in range(seqs):
-        fresh_state = (
-            columns[:, t : t + 1] * state_buf[t]
-            + columns[:, seqs + t : seqs + t + 1] * vec_in[t : t + 1]
-        )
-        new_state_ref[t] = fresh_state
-        value = jnp.sum(fresh_state * vec_read[t : t + 1], axis=1, keepdims=True)
-        read = jnp.where(read_lane == t, value, read)
+        for h in range(heads):
+            part = pl.ds(h * head_dim, head_dim)
+            fresh_state = (
+                keep_rows[h, pl.ds(t, 1)] * state_buf[t, part]
+                + columns[h * head_dim : (h + 1) * head_dim, t : t + 1]
+                * vec_in_rows[pl.ds(t, 1)]
+            )
+            new_state_ref[t, part] = fresh_state
+            value = lax.dot_general(
+                fresh_state.astype(bf16), read_rows, nt, preferred_element_type=f32
+            )
+            reads[h] = jnp.where(read_lane == t, value, reads[h])
+    read = jnp.concatenate(reads, axis=0)
+    read = jnp.concatenate([read, jnp.zeros((channels, channels - seqs), f32)], axis=1)
     read = read.T[0:seqs]
     gated = (read * (gate_z * jax.nn.sigmoid(gate_z)) * row(inner_ref)).astype(bf16)
     mix_own[...] = jnp.dot(gated, proj_out_ref[...], preferred_element_type=f32).astype(bf16)
@@ -266,8 +269,8 @@
         half_own.at[core], half_far.at[core], mix_send.at[1], mix_recv.at[1], me, across
     )
     over_x.start()
+    send_dense(1)
     send_dense(2)
-    sends += dense_copies
 
     over_x.wait_recv()
     to_core = remote(
@@ -315,46 +318,34 @@
     upper = my_z // (nz // 2)
     far_first = [other(upper * j + (1 - upper) * (nz - 2 - j)) for j in range(nz - 1)]
 
-    def rows_copy(k, at, send, ep_to, tp_to, k_to):
+    def rows_copy(k, at, ep_to, tp_to, k_to, side=None):
         return remote(
             rows_buf.at[k, at],
             rows_buf.at[k_to, at],
-            rows_send.at[send, at],
-            rows_recv.at[k_to, at],
+            rows_send,
+            rows_recv.at[k_to // 2, at] if k_to % 2 == 0 else side_recv.at[side],
             ep_to,
             tp_to,
         )
 
-    def aux_copy(at, send, ep_to):
-        return remote(
-            aux_buf.at[at], aux_buf.at[at], aux_send.at[send, at], aux_recv.at[at], ep_to, tp
-        )
+    def aux_copy(at, ep_to):
+        return remote(aux_buf.at[at], aux_buf.at[at], aux_send, aux_recv.at[at], ep_to, tp)
 
     def z_rows(z):
         return remote(
             rows_buf.at[0, here],
             rows_buf.at[0, here],
-            z_send.at[z],
+            rows_send,
             rows_recv.at[0, here],
             z * 2 + my_y,
             tp,
         )
 
-    def z_aux(z):
-        return remote(
-            aux_buf.at[here], aux_buf.at[here], z_aux_send.at[z], aux_recv.at[here],
-            z * 2 + my_y, tp,
-        )
-
-    def started(copy):
-        copy.start()
-        sends.append(copy)
-
     for z in far_first:
-        started(z_rows(z))
+        z_rows(z).start()
     over_y = my_z * 2 + 1 - my_y
-    started(rows_copy(0, here, 0, over_y, tp, 0))
-    started(rows_copy(2, here, 1, over_y, tp, 2))
+    rows_copy(0, here, over_y, tp, 0).start()
+    rows_copy(2, here, over_y, tp, 2).start()
 
     logits = lax.dot_general(
         feed, router_buf[...].astype(bf16), nt, preferred_element_type=f32
@@ -385,8 +376,8 @@
     pick = pick / jnp.sum(pick, axis=1, keepdims=True) * group_weight
     aux_buf[here] = jnp.where(lane == switch_lane, jax.nn.sigmoid(logits), pick).astype(bf16)
     for z in far_first:
-        started(z_aux(z))
-    started(aux_copy(here, 0, over_y))
+        aux_copy(here, z * 2 + my_y).start()
+    aux_copy(here, over_y).start()
 
     total = nz * seqs
     sides = (my_y, 1 - my_y)
@@ -395,40 +386,40 @@
         return sides[side] * nz + z
 
     def arrived(k, at):
-        rows_copy(k, at, 0, me, beside, k).wait_recv()
+        rows_copy(k, at, me, beside, k).wait_recv()
 
     there = at_of(1, my_z)
     for z in others:
         at = at_of(0, z)
         arrived(0, at)
-        started(rows_copy(0, at, 0, over_y, tp, 0))
-        started(rows_copy(0, at, 1, me, across, 2))
-        started(rows_copy(0, at, 2, me, beside, 1))
+        rows_copy(0, at, over_y, tp, 0).start()
+        rows_copy(0, at, me, across, 2).start()
+        rows_copy(0, at, me, beside, 1, 0).start()
     arrived(0, there)
-    started(rows_copy(0, there, 2, me, beside, 1))
+    rows_copy(0, there, me, beside, 1, 1).start()
     arrived(2, there)
-    started(rows_copy(2, there, 3, me, beside, 3))
+    rows_copy(2, there, me, beside, 3, 1).start()
     for z in others:
         at = at_of(0, z)
-        aux_copy(at, 0, me).wait_recv()
-        started(aux_copy(at, 0, over_y))
+        aux_copy(at, me).wait_recv()
+        aux_copy(at, over_y).start()
     for z in others:
         at = at_of(1, z)
         arrived(0, at)
-        started(rows_copy(0, at, 1, me, across, 2))
-        started(rows_copy(0, at, 2, me, beside, 1))
+        rows_copy(0, at, me, across, 2).start()
+        rows_copy(0, at, me, beside, 1, 1).start()
     for z in others:
         at = at_of(0, z)
         arrived(2, at)
-        started(rows_copy(2, at, 3, me, beside, 3))
+        rows_copy(2, at, me, beside, 3, 0).start()
 
     def gather_end(side):
         for z in range(nz) if side else others:
             at = at_of(side, z)
             if side:
-                aux_copy(at, 0, me).wait_recv()
-            arrived(1, at)
-            arrived(3, at)
+                aux_copy(at, me).wait_recv()
+        blocks = rows_buf.at[0:2, 0 : nz if side else nz - 1]
+        remote(blocks, blocks, rows_send, side_recv.at[side], me, beside).wait_recv()
 
     def add(total_sum, value):
         return value if total_sum is None else total_sum + value
@@ -438,7 +429,7 @@
         return remote(
             part_buf.at[(diagonal, beside)[k], block],
             part_peer.at[k, block],
-            part_send.at[k, side],
+            part_send,
             part_recv.at[k, side],
             me,
             beside,
@@ -468,12 +459,12 @@
             )
             part_buf[q, block] = value.astype(bf16).reshape(nz, seqs, quarter)
             if k < 2:
-                started(part_copy(k, side))
+                part_copy(k, side).start()
 
     far_then_own = far_first + [my_z]
 
     def x_copy(at):
-        return remote(send_x.at[at], recv_x.at[at], x_send.at[at], x_recv.at[at], me, across)
+        return remote(send_x.at[at], recv_x.at[at], x_send, x_recv.at[at], me, across)
 
     def sums_over_x(side):
         part_copy(0, side).wait_recv()
@@ -482,11 +473,11 @@
             send_x[at] = (
                 part_buf[across, at].astype(f32) + part_peer[0, at].astype(f32)
             ).astype(bf16)
-            started(x_copy(at))
+            x_copy(at).start()
 
     def ep_copy(at, slot, ep_to):
         return remote(
-            send_ep.at[at], recv_ep.at[slot], ep_send.at[at], ep_recv.at[slot], ep_to, tp
+            send_ep.at[at], recv_ep.at[slot], ep_send, ep_recv, ep_to, tp
         )
 
     def summed(at):
@@ -502,18 +493,21 @@
         for z in far_then_own if side else far_first:
             at = at_of(side, z)
             send_ep[at] = summed(at).astype(bf16)
-            started(ep_copy(at, here, z * 2 + sides[side]))
-
-    for copy in local[5:]:
-        copy.wait()
-    for copy in dense_copies:
-        copy.wait_recv()
+            ep_copy(at, here, z * 2 + sides[side]).start()
+
+    loaded(gate_w, 5)
+    loaded(up_w, 6)
+    loaded(down_w, 7)
+    loaded(dense_w.at[:, tp], 8)
+    others_dense = dense_w.at[:, 0:3]
+    all_dense = remote(others_dense, others_dense, dense_send, dense_recv, me, beside)
+    all_dense.wait_recv()
     gather_end(0)
     feed_forward(0)
     for z in others:
         at = at_of(1, z)
         arrived(2, at)
-        started(rows_copy(2, at, 3, me, beside, 3))
+        rows_copy(2, at, me, beside, 3, 1).start()
     sums_over_x(0)
     gather_end(1)
     feed_forward(1)
@@ -522,11 +516,11 @@
     combined = summed(here)
     sums_over_ep(1)
 
+    seven = pl.ds(0, ep - 1)
+    remote(send_ep.at[seven], recv_ep.at[seven], ep_send, ep_recv, me, beside).wait_recv()
     for side in range(2):
         for z in range(nz) if side else others:
-            at = at_of(side, z)
-            ep_copy(at, at, me).wait_recv()
-            combined = combined + recv_ep[at].astype(f32)
+            combined = combined + recv_ep[at_of(side, z)].astype(f32)
 
     square = jnp.sum(combined * combined, axis=1, keepdims=True)
     lanes = square_own.shape[1]
@@ -534,16 +528,10 @@
     diagonal_lane = row_id == lax.broadcasted_iota(jnp.int32, (seqs, lanes), 1)
     square_row = jnp.sum(jnp.where(diagonal_lane, square, 0.0), axis=0, keepdims=True)
     square_own[...] = jnp.broadcast_to(square_row, square_own.shape)
-    square_copies = []
     for k, peer in enumerate(near):
-        copy = remote(
-            square_own, square_peer.at[k], square_send.at[k], square_recv.at[k], me, peer
-        )
-        copy.start()
-        square_copies.append(copy)
-    sends += square_copies
-    for copy in square_copies:
-        copy.wait_recv()
+        remote(square_own, square_peer.at[k], square_send, square_recv, me, peer).start()
+    all_squares = remote(square_peer, square_peer, square_send, square_recv, me, beside)
+    all_squares.wait_recv()
     everything = (square_own[...] + square_peer[0]) + (square_peer[1] + square_peer[2])
     spread = jnp.where(diagonal_lane, everything[0:1], 0.0)
     scale = lax.rsqrt(jnp.sum(spread, axis=1, keepdims=True) / width + norm_eps)
@@ -551,6 +539,17 @@
     out_ref[...] = (own_stream + combined * scale * row(out_gain_ref)).astype(bf16)
     for copy in sends:
         copy.wait_send()
+    blocks = rows_buf.at[:, seven]
+    for ref, sem in (
+        (blocks, rows_send),
+        (aux_buf.at[seven], aux_send),
+        (part_peer, part_send),
+        (send_x, x_send),
+        (send_ep.at[seven], ep_send),
+    ):
+        remote(ref, ref, sem, mix_recv.at[0], me, beside).wait_send()
+    all_dense.wait_send()
+    all_squares.wait_send()
 
 
 def write_kernel(out_ref, state_ref, conv_ref, out_hbm, state_hbm, conv_hbm, sems):
@@ -622,13 +621,13 @@
         scratch_shapes=[
             pltpu.VMEM((4,) + proj_x.shape, bf16),
             pltpu.VMEM(state.shape, state.dtype),
+            pltpu.VMEM((step_bias.shape[0], seqs, channels), jnp.float32),
+            pltpu.VMEM((seqs, channels), jnp.float32),
             pltpu.VMEM((lanes, width), jnp.float32),
             pltpu.VMEM((width, hidden_here), bf16),
             pltpu.VMEM((width, hidden_here), bf16),
             pltpu.VMEM((4, hidden_here, quarter), bf16),
-            pltpu.VMEM((4, share, quarter), bf16),
-            pltpu.VMEM((4, share, quarter), bf16),
-            pltpu.VMEM((4, share, quarter), bf16),
+            pltpu.VMEM((3, 4, share, quarter), bf16),
             pltpu.VMEM((4, seqs, quarter), bf16),
             pltpu.VMEM((seqs, width), bf16),
             pltpu.VMEM((seqs, width), bf16),
@@ -644,26 +643,25 @@
             pltpu.VMEM((ep, seqs, quarter), bf16),
             pltpu.VMEM((8, lanes), jnp.float32),
             pltpu.VMEM((3, 8, lanes), jnp.float32),
-            dma((14,)),
             dma((9,)),
-            dma((9,)),
+            dma,
+            dma,
             dma((3,)),
             dma((3,)),
-            dma((4, ep)),
-            dma((4, ep)),
-            dma((1, ep)),
+            dma,
+            dma((2, ep)),
+            dma,
             dma((ep,)),
+            dma,
             dma((2, 2)),
-            dma((2, 2)),
+            dma,
             dma((ep,)),
-            dma((ep,)),
-            dma((ep,)),
-            dma((ep,)),
-            dma((3,)),
-            dma((3,)),
+            dma,
+            dma,
+            dma,
+            dma,
             pltpu.SemaphoreType.REGULAR,
-            dma((ep,)),
-            dma((ep,)),
+            dma((2,)),
         ],
         compiler_params=pltpu.CompilerParams(collective_id=0, has_side_effects=True),
         name="fused_layer",

time: 47 us -> 43.2 us (0.919)
  Pallas kernels: 46.2 us -> 42.4 us
    pallas_call x1, Pallas kernels: 44.9 us -> 41 us  [fused_layer(): pl.pallas_call(kernel, out_shape=(pltpu.VMEM((seqs, quarter), bf16), pltp...]
where the time goes in v3:
time: 43.2 us; the launch traced here: 43 us
  Pallas kernels  42.4 us (98%)
  between operations  0.65 us (2%)
    pallas_call x1, Pallas kernels, fused_layer(): pl.pallas_call(kernel, out_shape=(pltpu.VMEM((seqs, quarter), bf16), pltp...  41 us
    pallas_call x1, Pallas kernels, fused_layer(): pl.pallas_call(write_kernel, out_shape=tuple((jax.ShapeDtypeStruct(one.sh...  1.36 us

profile of v3, /device:TPU:0, one launch (start us, length us, event | category | flops | bytes accessed | tf_op | source)
XLA Modules:
  0.0 43.0 jit_solution(3982388075257964923)
XLA Ops:
  0.6 41.0 %fused_layer.1 = (bf16[32,512]{1,0:T(8,128)(2,1)S(1)}, f32[32,128,128]{2,1,0:T(8,128)S(1)}, bf16[3,3,32,128]{3,2,1,0:T(8,128)(2,1)S(1)}) custom-call(bf16[128,2048]{1,0:T(8,128)(2,1)} %proj_out_ref.1, bf16[32,2048]{1,0:T(8,128)(2,1)} %resid_ref.1, bf16[2048]{0:T(1024)(128)(2,1)} %mix_ref.1, bf16[2048]{0:T(1024)(128)(2,1)} %post_ref.1, ...), custom_call_target="tpu_custom_call" | custom-call | tf_op jit(solution)/shard_map/fused_layer/pallas_call | solution.py:612
  41.7 1.4 %write_results.1 = (bf16[32,512]{1,0:T(8,128)(2,1)}, f32[32,128,128]{2,1,0:T(8,128)}, bf16[3,3,32,128]{3,2,1,0:T(8,128)(2,1)}) custom-call(bf16[32,512]{1,0:T(8,128)(2,1)S(1)} %get-tuple-element.9.out_ref, f32[32,128,128]{2,1,0:T(8,128)S(1)} %get-tuple-element.10.state_ref, bf16[3,3,32,128]{3,2,1,0:T(8,128)(2,1)S(1)} %get-tuple-element.11.conv_ref), custom_call_target="tpu_custom_call" | custom-call | tf_op jit(solution)/shard_map/write_results/pallas_call | solution.py:697

commit v4 on v3

--- a/solution.py
+++ b/solution.py
@@ -26,22 +26,22 @@
     group_size,
     group_count,
     expert_count,
-    proj_out_ref,
-    resid_ref,
-    mix_ref,
-    post_ref,
-    ffn_ref,
-    expert_router_ref,
-    group_router_ref,
-    switch_ref,
-    route_ref,
-    out_gain_ref,
-    inner_ref,
-    proj_step_ref,
-    taps_ref,
-    conv_ref,
-    bias_ref,
-    decay_ref,
+    proj_out_hbm,
+    resid_hbm,
+    mix_hbm,
+    post_hbm,
+    ffn_hbm,
+    expert_router_hbm,
+    group_router_hbm,
+    switch_hbm,
+    route_hbm,
+    out_gain_hbm,
+    inner_hbm,
+    proj_step_hbm,
+    taps_hbm,
+    conv_hbm,
+    bias_hbm,
+    decay_hbm,
     proj_x_hbm,
     proj_z_hbm,
     proj_b_hbm,
@@ -99,6 +99,23 @@
     square_recv,
     entered,
     side_recv,
+    small_sem,
+    proj_out_ref,
+    resid_ref,
+    mix_ref,
+    post_ref,
+    ffn_ref,
+    expert_router_ref,
+    group_router_ref,
+    switch_ref,
+    route_ref,
+    out_gain_ref,
+    inner_ref,
+    proj_step_ref,
+    taps_ref,
+    conv_ref,
+    bias_ref,
+    decay_ref,
 ):
     f32, bf16 = jnp.float32, jnp.bfloat16
     me = lax.axis_index("ep")
@@ -111,8 +128,8 @@
     near = (beside, across, diagonal)
     seqs, width = resid_ref.shape
     quarter = width // 4
-    share = dense_w.shape[2]
-    dgate, dup, ddown = dense_w.at[0], dense_w.at[1], dense_w.at[2]
+    share = dense_w.shape[1]
+    dense_at = (tp * 2, tp * 2 + 1, tp + 8)
 
     def remote(src, dst, send, recv, ep_to, tp_to):
         return pltpu.make_async_remote_copy(
@@ -127,23 +144,6 @@
     def ep_at(step):
         return lax.rem(me + step + ep, ep)
 
-    def load(src, dst, at):
-        pltpu.make_async_copy(src, dst, local_sem.at[at]).start()
-
-    def loaded(dst, at):
-        pltpu.make_async_copy(dst, dst, local_sem.at[at]).wait()
-
-    for k, src in enumerate((proj_x_hbm, proj_b_hbm, proj_c_hbm, proj_z_hbm)):
-        load(src, proj_w.at[k], k)
-    load(state_hbm, state_buf, 4)
-    load(gate_hbm.at[0], gate_w, 5)
-    load(up_hbm.at[0], up_w, 6)
-    for q in range(4):
-        load(down_hbm.at[0, :, pl.ds(q * quarter, quarter)], down_w.at[q], 7)
-    dense_pairs = ((dense_gate_hbm, dgate), (dense_up_hbm, dup), (dense_down_hbm, ddown))
-    for src, dst in dense_pairs:
-        load(src.at[pl.ds(tp * share, share), :], dst.at[tp], 8)
-
     barrier = pltpu.get_barrier_semaphore()
     for step in range(1, ep):
 
@@ -158,49 +158,91 @@
             barrier, inc=1, device_id=(me, peer), device_id_type=pl.DeviceIdType.MESH
         )
 
+    def load(src, dst, at):
+        pltpu.make_async_copy(src, dst, local_sem.at[at]).start()
+
+    def loaded(dst, at):
+        pltpu.make_async_copy(dst, dst, local_sem.at[at]).wait()
+
+    small_pairs = (
+        (resid_hbm, resid_ref),
+        (mix_hbm, mix_ref),
+        (proj_step_hbm, proj_step_ref),
+        (taps_hbm, taps_ref),
+        (conv_hbm, conv_ref),
+        (bias_hbm, bias_ref),
+        (decay_hbm, decay_ref),
+        (inner_hbm, inner_ref),
+        (proj_out_hbm, proj_out_ref),
+        (post_hbm, post_ref),
+        (ffn_hbm, ffn_ref),
+        (expert_router_hbm, expert_router_ref),
+        (group_router_hbm, group_router_ref),
+        (switch_hbm, switch_ref),
+        (route_hbm, route_ref),
+        (out_gain_hbm, out_gain_ref),
+    )
+    small_copies = [
+        pltpu.make_async_copy(src, dst, small_sem.at[k])
+        for k, (src, dst) in enumerate(small_pairs)
+    ]
+    for copy in small_copies[:5]:
+        copy.start()
+    for k, src in enumerate((proj_x_hbm, proj_b_hbm, proj_c_hbm, proj_z_hbm)):
+        load(src, proj_w.at[k], k)
+    load(state_hbm, state_buf, 4)
+    for copy in small_copies[5:]:
+        copy.start()
+    dense_srcs = (dense_gate_hbm, dense_up_hbm, dense_down_hbm)
+
     def row(ref):
         return ref[...].astype(f32).reshape(1, ref.shape[0])
 
+    pl.semaphore_wait(barrier, me + 3)
+    for step in range(1, ep):
+
+        @pl.when(me >= step)
+        def _():
+            pl.semaphore_signal(
+                entered, inc=1, device_id=(me - step, tp), device_id_type=pl.DeviceIdType.MESH
+            )
+
+
+    sends = []
+
+    def send_dense(t):
+        src, dst = dense_srcs[t], dense_w.at[dense_at[t]]
+        for peer in near:
+            remote(
+                src.at[pl.ds(peer * share, share), :],
+                dst,
+                dense_send,
+                dense_recv,
+                me,
+                peer,
+            ).start()
+
+    send_dense(0)
+
+    @pl.when(core == 0)
+    def _():
+        send_dense(1)
+
+
+    for copy in small_copies[:3]:
+        copy.wait()
     resid_f = resid_ref[...].astype(f32)
     resid_scale = lax.rsqrt(jnp.mean(resid_f * resid_f, axis=1, keepdims=True) + norm_eps)
     normed = (resid_f * resid_scale * row(mix_ref)).astype(bf16)
     group_base = -(-expert_count // 8) * 8
     switch_lane = group_base + -(-group_count // 8) * 8
-    router_buf[...] = jnp.zeros_like(router_buf)
-    router_buf[0:expert_count, :] = expert_router_ref[...].astype(f32)
-    router_buf[group_base : group_base + group_count, :] = group_router_ref[...].astype(f32)
-    router_buf[switch_lane : switch_lane + 1, :] = row(switch_ref)
     nt = (((1,), (1,)), ((), ()))
     step_all = lax.dot_general(normed, proj_step_ref[...], nt, preferred_element_type=f32)
-    pl.semaphore_wait(barrier, me + 3)
-    for step in range(1, ep):
-
-        @pl.when(me >= step)
-        def _():
-            pl.semaphore_signal(
-                entered, inc=1, device_id=(me - step, tp), device_id_type=pl.DeviceIdType.MESH
-            )
-
-
-    sends = []
-
-    def send_dense(t):
-        src, dst = dense_pairs[t]
-        for peer in near:
-            remote(
-                src.at[pl.ds(peer * share, share), :],
-                dst.at[tp],
-                dense_send,
-                dense_recv,
-                me,
-                peer,
-            ).start()
-
-    send_dense(0)
-
     channels = conv_ref.shape[3]
     heads = bias_ref.shape[0]
     head_dim = channels // heads
+    for copy in small_copies[3:7]:
+        copy.wait()
     taps = taps_ref[...].astype(f32)
     old = conv_ref.shape[1]
     active = []
@@ -235,7 +277,15 @@
     ).T
     vec_in_rows[...] = vec_in
     read_rows = vec_read.astype(bf16)
+    for copy in small_copies[7:]:
+        copy.wait()
     loaded(state_buf, 4)
+    load(gate_hbm.at[0], gate_w, 5)
+    load(up_hbm.at[0], up_w, 6)
+    for q in range(4):
+        load(down_hbm.at[0, :, pl.ds(q * quarter, quarter)], down_w.at[q], 7)
+    for src, at in zip(dense_srcs, dense_at):
+        load(src.at[pl.ds(tp * share, share), :], dense_w.at[at], 8)
     read_lane = lax.broadcasted_iota(jnp.int32, (head_dim, seqs), 1)
     reads = [jnp.zeros((head_dim, seqs), f32) for h in range(heads)]
     for t in range(seqs):
@@ -265,20 +315,32 @@
     chip_sum = (mix_own[...].astype(f32) + mix_peer[...].astype(f32)).astype(bf16)
     half_own[0] = chip_sum[:, :half]
     half_own[1] = chip_sum[:, half:]
-    over_x = remote(
-        half_own.at[core], half_far.at[core], mix_send.at[1], mix_recv.at[1], me, across
-    )
-    over_x.start()
-    send_dense(1)
-    send_dense(2)
-
-    over_x.wait_recv()
-    to_core = remote(
-        half_far.at[core], half_far.at[core], mix_send.at[2], mix_recv.at[2], me, beside
-    )
-    to_core.start()
-    sends += [over_x, to_core]
-    to_core.wait_recv()
+
+    def far_half(h, tp_to, src):
+        return remote(src.at[h], half_far.at[h], mix_send.at[1], mix_recv.at[1 + h], me, tp_to)
+
+    @pl.when(core == 1)
+    def _():
+        for h in range(2):
+            far_half(h, across, half_own).start()
+        send_dense(1)
+        send_dense(2)
+
+    router_buf[...] = jnp.zeros_like(router_buf)
+    router_buf[0:expert_count, :] = expert_router_ref[...].astype(f32)
+    router_buf[group_base : group_base + group_count, :] = group_router_ref[...].astype(f32)
+    router_buf[switch_lane : switch_lane + 1, :] = row(switch_ref)
+
+    for h in range(2):
+        far_half(h, across, half_own).wait_recv()
+
+        @pl.when(core == 1)
+        def _():
+            far_half(h, beside, half_far).start()
+
+    @pl.when(core == 0)
+    def _():
+        send_dense(2)
 
     far_sum = jnp.concatenate([half_far[0], half_far[1]], axis=1)
     mixed = chip_sum.astype(f32) + far_sum.astype(f32)
@@ -328,8 +390,9 @@
             tp_to,
         )
 
-    def aux_copy(at, ep_to):
-        return remote(aux_buf.at[at], aux_buf.at[at], aux_send, aux_recv.at[at], ep_to, tp)
+    def aux_copy(side, ep_to):
+        mine = aux_buf.at[here]
+        return remote(mine, mine, aux_send, aux_recv.at[side], ep_to, tp)
 
     def z_rows(z):
         return remote(
@@ -347,6 +410,25 @@
     rows_copy(0, here, over_y, tp, 0).start()
     rows_copy(2, here, over_y, tp, 2).start()
 
+    total = nz * seqs
+    sides = (my_y, 1 - my_y)
+
+    def at_of(side, z):
+        return sides[side] * nz + z
+
+    def arrived(k, at):
+        rows_copy(k, at, me, beside, k).wait_recv()
+
+    there = at_of(1, my_z)
+    def gather_z(z):
+        at = at_of(0, z)
+        arrived(0, at)
+        rows_copy(0, at, over_y, tp, 0).start()
+        rows_copy(0, at, me, across, 2).start()
+        rows_copy(0, at, me, beside, 1, 0).start()
+
+    for z in others[:-1]:
+        gather_z(z)
     logits = lax.dot_general(
         feed, router_buf[...].astype(bf16), nt, preferred_element_type=f32
     )
@@ -376,33 +458,14 @@
     pick = pick / jnp.sum(pick, axis=1, keepdims=True) * group_weight
     aux_buf[here] = jnp.where(lane == switch_lane, jax.nn.sigmoid(logits), pick).astype(bf16)
     for z in far_first:
-        aux_copy(here, z * 2 + my_y).start()
-    aux_copy(here, over_y).start()
-
-    total = nz * seqs
-    sides = (my_y, 1 - my_y)
-
-    def at_of(side, z):
-        return sides[side] * nz + z
-
-    def arrived(k, at):
-        rows_copy(k, at, me, beside, k).wait_recv()
-
-    there = at_of(1, my_z)
-    for z in others:
-        at = at_of(0, z)
-        arrived(0, at)
-        rows_copy(0, at, over_y, tp, 0).start()
-        rows_copy(0, at, me, across, 2).start()
-        rows_copy(0, at, me, beside, 1, 0).start()
+        aux_copy(0, z * 2 + my_y).start()
+    for z in far_first + [my_z]:
+        aux_copy(1, z * 2 + 1 - my_y).start()
+    gather_z(others[-1])
     arrived(0, there)
     rows_copy(0, there, me, beside, 1, 1).start()
     arrived(2, there)
     rows_copy(2, there, me, beside, 3, 1).start()
-    for z in others:
-        at = at_of(0, z)
-        aux_copy(at, me).wait_recv()
-        aux_copy(at, over_y).start()
     for z in others:
         at = at_of(1, z)
         arrived(0, at)
@@ -414,11 +477,10 @@
         rows_copy(2, at, me, beside, 3, 0).start()
 
     def gather_end(side):
-        for z in range(nz) if side else others:
-            at = at_of(side, z)
-            if side:
-                aux_copy(at, me).wait_recv()
-        blocks = rows_buf.at[0:2, 0 : nz if side else nz - 1]
+        count = nz if side else nz - 1
+        aux = aux_buf.at[0:count]
+        remote(aux, aux, aux_send, aux_recv.at[side], me, beside).wait_recv()
+        blocks = rows_buf.at[0:2, 0:count]
         remote(blocks, blocks, rows_send, side_recv.at[side], me, beside).wait_recv()
 
     def add(total_sum, value):
@@ -437,16 +499,15 @@
 
     def feed_forward(side):
         block = pl.ds(sides[side] * nz, nz)
-        gate = up = dense_g = dense_u = None
+        gate = up = dense = None
         for k, q in enumerate(quarters):
             rows = rows_buf[k, block].reshape(total, quarter)
             span = pl.ds(pl.multiple_of(q * quarter, quarter), quarter)
             gate = add(gate, jnp.dot(rows, gate_w[span, :], preferred_element_type=f32))
             up = add(up, jnp.dot(rows, up_w[span, :], preferred_element_type=f32))
-            dense_g = add(
-                dense_g, lax.dot_general(rows, dgate[q], nt, preferred_element_type=f32)
-            )
-            dense_u = add(dense_u, lax.dot_general(rows, dup[q], nt, preferred_element_type=f32))
+            pair = dense_w[pl.ds(q * 2, 2)].reshape(2 * share, quarter)
+            dense = add(dense, lax.dot_general(rows, pair, nt, preferred_element_type=f32))
+        dense_g, dense_u = dense[:, :share], dense[:, share:]
         aux = aux_buf[block].reshape(total, aux_buf.shape[2]).astype(f32)
         aux_lane = lax.broadcasted_iota(jnp.int32, aux.shape, 1)
         weight = jnp.sum(jnp.where(aux_lane == me, aux, 0.0), axis=1, keepdims=True)
@@ -455,7 +516,7 @@
         dense_hidden = (dense_g * jax.nn.sigmoid(dense_g) * dense_u * switch).astype(bf16)
         for k, q in enumerate((diagonal, beside, across, tp)):
             value = jnp.dot(hidden, down_w[q], preferred_element_type=f32) + jnp.dot(
-                dense_hidden, ddown[q], preferred_element_type=f32
+                dense_hidden, dense_w[q + 8], preferred_element_type=f32
             )
             part_buf[q, block] = value.astype(bf16).reshape(nz, seqs, quarter)
             if k < 2:
@@ -498,8 +559,8 @@
     loaded(gate_w, 5)
     loaded(up_w, 6)
     loaded(down_w, 7)
-    loaded(dense_w.at[:, tp], 8)
-    others_dense = dense_w.at[:, 0:3]
+    loaded(dense_w.at[0:3], 8)
+    others_dense = dense_w.at[0:9]
     all_dense = remote(others_dense, others_dense, dense_send, dense_recv, me, beside)
     all_dense.wait_recv()
     gather_end(0)
@@ -511,8 +572,8 @@
     sums_over_x(0)
     gather_end(1)
     feed_forward(1)
+    sums_over_x(1)
     sums_over_ep(0)
-    sums_over_x(1)
     combined = summed(here)
     sums_over_ep(1)
 
@@ -549,6 +610,12 @@
     ):
         remote(ref, ref, sem, mix_recv.at[0], me, beside).wait_send()
     all_dense.wait_send()
+
+    @pl.when(core == 1)
+    def _():
+        halves = rows_buf.at[0:2, 0:4]
+        remote(halves, halves, mix_send.at[1], mix_recv.at[0], me, beside).wait_send()
+
     all_squares.wait_send()
 
 
@@ -606,7 +673,6 @@
     kernel = functools.partial(
         fused_kernel, ep, expert_count // group_count, group_count, expert_count
     )
-    smem = pl.BlockSpec(memory_space=pltpu.SMEM)
     earlier = conv_state.transpose(1, 2, 0, 3)
     state = scan_state.reshape(seqs, channels, scan_state.shape[3])
     results = pl.pallas_call(
@@ -616,7 +682,7 @@
             pltpu.VMEM(state.shape, state.dtype),
             pltpu.VMEM(earlier.shape, earlier.dtype),
         ),
-        in_specs=[vmem] * 14 + [smem] * 2 + [hbm] * 11,
+        in_specs=[hbm] * 27,
         out_specs=(vmem, vmem, vmem),
         scratch_shapes=[
             pltpu.VMEM((4,) + proj_x.shape, bf16),
@@ -627,7 +693,7 @@
             pltpu.VMEM((width, hidden_here), bf16),
             pltpu.VMEM((width, hidden_here), bf16),
             pltpu.VMEM((4, hidden_here, quarter), bf16),
-            pltpu.VMEM((3, 4, share, quarter), bf16),
+            pltpu.VMEM((12, share, quarter), bf16),
             pltpu.VMEM((4, seqs, quarter), bf16),
             pltpu.VMEM((seqs, width), bf16),
             pltpu.VMEM((seqs, width), bf16),
@@ -646,12 +712,12 @@
             dma((9,)),
             dma,
             dma,
-            dma((3,)),
+            dma((2,)),
             dma((3,)),
             dma,
             dma((2, ep)),
             dma,
-            dma((ep,)),
+            dma((2,)),
             dma,
             dma((2, 2)),
             dma,
@@ -662,6 +728,23 @@
             dma,
             pltpu.SemaphoreType.REGULAR,
             dma((2,)),
+            dma((16,)),
+            pltpu.VMEM(proj_out.shape, proj_out.dtype),
+            pltpu.VMEM(resid.shape, resid.dtype),
+            pltpu.VMEM(mix_gain.shape, mix_gain.dtype),
+            pltpu.VMEM(post_gain.shape, post_gain.dtype),
+            pltpu.VMEM(ffn_gain.shape, ffn_gain.dtype),
+            pltpu.VMEM(expert_router.T.shape, expert_router.T.dtype),
+            pltpu.VMEM(group_router.T.shape, group_router.T.dtype),
+            pltpu.VMEM(dense_switch.shape, dense_switch.dtype),
+            pltpu.VMEM(route_experts.T.shape, route_experts.T.dtype),
+            pltpu.VMEM(out_gain.shape, out_gain.dtype),
+            pltpu.VMEM(inner_gain.shape, inner_gain.dtype),
+            pltpu.VMEM(proj_step.T.shape, proj_step.T.dtype),
+            pltpu.VMEM(conv_taps.shape, conv_taps.dtype),
+            pltpu.VMEM(earlier.shape, earlier.dtype),
+            pltpu.SMEM(step_bias.shape, step_bias.dtype),
+            pltpu.SMEM(decay_rate.shape, decay_rate.dtype),
         ],
         compiler_params=pltpu.CompilerParams(collective_id=0, has_side_effects=True),
         name="fused_layer",

time: 43.2 us -> 40.3 us (0.933)
  Pallas kernels: 42.4 us -> 39.5 us
    pallas_call x1, Pallas kernels: 41 us -> 38.1 us  [fused_layer(): pl.pallas_call(kernel, out_shape=(pltpu.VMEM((seqs, quarter), bf16), pltp...]
where the time goes in v4:
time: 40.3 us; the launch traced here: 40.1 us
  Pallas kernels  39.5 us (98%)
  between operations  0.65 us (2%)
    pallas_call x1, Pallas kernels, fused_layer(): pl.pallas_call(kernel, out_shape=(pltpu.VMEM((seqs, quarter), bf16), pltp...  38.1 us
    pallas_call x1, Pallas kernels, fused_layer(): pl.pallas_call(write_kernel, out_shape=tuple((jax.ShapeDtypeStruct(one.sh...  1.36 us

profile of v4, /device:TPU:0, one launch (start us, length us, event | category | flops | bytes accessed | tf_op | source)
XLA Modules:
  0.0 40.1 jit_solution(8836773121831280622)
XLA Ops:
  0.6 38.1 %fused_layer.1 = (bf16[32,512]{1,0:T(8,128)(2,1)S(1)}, f32[32,128,128]{2,1,0:T(8,128)S(1)}, bf16[3,3,32,128]{3,2,1,0:T(8,128)(2,1)S(1)}) custom-call(bf16[128,2048]{1,0:T(8,128)(2,1)} %proj_out_hbm.1, bf16[32,2048]{1,0:T(8,128)(2,1)} %resid_hbm.1, bf16[2048]{0:T(1024)(128)(2,1)} %mix_hbm.1, bf16[2048]{0:T(1024)(128)(2,1)} %post_hbm.1, ...), custom_call_target="tpu_custom_call" | custom-call | tf_op jit(solution)/shard_map/fused_layer/pallas_call | solution.py:678
  38.8 1.4 %write_results.1 = (bf16[32,512]{1,0:T(8,128)(2,1)}, f32[32,128,128]{2,1,0:T(8,128)}, bf16[3,3,32,128]{3,2,1,0:T(8,128)(2,1)}) custom-call(bf16[32,512]{1,0:T(8,128)(2,1)S(1)} %get-tuple-element.9.out_ref, f32[32,128,128]{2,1,0:T(8,128)S(1)} %get-tuple-element.10.state_ref, bf16[3,3,32,128]{3,2,1,0:T(8,128)(2,1)S(1)} %get-tuple-element.11.conv_ref), custom_call_target="tpu_custom_call" | custom-call | tf_op jit(solution)/shard_map/write_results/pallas_call | solution.py:780
